TPU v7x, 512 devices: a whole 4x4x16 slice. The times are simulated.
512 devices in a mesh: kv: 128 (over z, x, core), tp: 4 (over y).
Axes of the slice: x: 4, y: 4, z: 16, core: 2. Of those that a mesh axis runs over, the one named last changes fastest.
Arguments:
- tokens: bfloat16 [16384, 2048], P('kv'), may hold values from -64 to 64
- query_weight: bfloat16 [2048, 1024], P(None, 'tp'), may hold values from -0.125 to 0.125
- key_weight: bfloat16 [2048, 256], P(None, 'tp'), may hold values from -0.125 to 0.125
- value_weight: bfloat16 [2048, 256], P(None, 'tp'), may hold values from -0.125 to 0.125
- out_weight: bfloat16 [1024, 2048], P(None, 'tp'), may hold values from -0.1875 to 0.1875
- alibi_slope: float32 [16], P('tp'), may hold values from 1.5258789e-05 to 0.03
- block_choice: int32 [512, 8], P('kv'), may hold values from -1 to 511, as said below
Outputs:
- mixed: bfloat16 [16384, 2048], P('kv', 'tp')
Inputs may be any that keep to these rules, and one draw needn't show every extreme that they name: `block_choice`: row g begins with g; its other entries are distinct blocks below g, or -1 where nothing is chosen. The rows of one index of kv (aligned runs of 4 rows) together name at most one block of any other index of kv, and some rows of each index name a block of the index before it and of the index half the axis before it where those exist.
All inputs are finite; a program needn't handle non-finite values.
Results may differ from a plain program's by a relative error of at most 0.012.
Values may be sent and summed in bfloat16 or wider, within the bound.
No kernel may reach another device: no remote copies, remote signals or barrier semaphores. Data moves between devices by JAX's collectives and lax.ppermute only.
A program may use at most 64 MiB of HBM per device.

v0:
```python
import jax
import jax.numpy as jnp
from jax import lax
from jax.sharding import Mesh
from jax.sharding import PartitionSpec as P

HEAD = 64
BLOCK = 32
KV = ("kv_0", "kv_1", "kv_2")


def cut_along(value, dim, peers):
    before, after = (value.shape[:dim], value.shape[dim + 1 :])
    return jnp.moveaxis(value.reshape(*before, peers, -1, *after), dim, 0)


def laid_out(tiles, dim):
    tiles = jnp.moveaxis(tiles, 0, dim)
    lengths = tiles.shape
    return tiles.reshape(*lengths[:dim], lengths[dim] * lengths[dim + 1], *lengths[dim + 2 :])


def exchange_in_order(tiles, axes, order):
    lengths = [lax.axis_size(a) for a in axes]
    tiles = tiles.reshape(*lengths, *tiles.shape[1:])
    for k in order:
        tiles = lax.all_to_all(tiles, axes[k], split_axis=k, concat_axis=k, tiled=True)
    return tiles.reshape(-1, *tiles.shape[len(axes) :])


def core_and_chips(value, groups, order, split_dim, concat_dim):
    peers = lax.axis_size(groups[0]) * lax.axis_size(groups[1])
    tiles = cut_along(value, split_dim, peers)
    return laid_out(exchange_in_order(tiles, groups, order), concat_dim)


def copy_for_each(value, axis):
    peers = lax.axis_size(axis)
    return lax.all_to_all(
        jnp.broadcast_to(value[None], (peers, *value.shape)), axis, 0, 0, tiled=True
    )


def collect(value, axis, dim):
    return laid_out(copy_for_each(value, axis), dim)


def shards(tokens, query_weight, key_weight, value_weight, out_weight, alibi_slope, block_choice):
    rows = tokens.shape[0]
    blocks_here = rows // BLOCK
    n_kv = lax.axis_size(KV)
    device = lax.axis_index(KV)
    queries = jnp.dot(tokens, query_weight, preferred_element_type=jnp.float32).astype(jnp.bfloat16)
    keys = jnp.dot(tokens, key_weight, preferred_element_type=jnp.float32).astype(jnp.bfloat16)
    values = jnp.dot(tokens, value_weight, preferred_element_type=jnp.float32).astype(jnp.bfloat16)
    packed = jnp.concatenate([keys, values], axis=1)
    safe_ids = jnp.maximum(block_choice, 0)
    owners = safe_ids // blocks_here
    local_index = safe_ids % blocks_here
    remote = (block_choice >= 0) & (owners != device)
    match = remote[..., None] & (owners[..., None] == jnp.arange(n_kv, dtype=jnp.int32))
    wanted = jnp.max(jnp.where(match, local_index[..., None], -1), axis=(0, 1))
    own_blocks = packed.reshape(blocks_here, BLOCK, 2 * HEAD)
    asked = core_and_chips(wanted.reshape(n_kv, 1), (("kv_0", "kv_1"), "kv_2"), (1, 0), 0, 0)
    outgoing = own_blocks[jnp.clip(asked[:, 0], 0, blocks_here - 1)]
    incoming = lax.all_to_all(outgoing, KV, split_axis=0, concat_axis=0, tiled=True)
    table = jnp.concatenate([own_blocks, incoming], axis=0)
    slot_ids = jnp.where(owners == device, local_index, blocks_here + owners)
    selected = table[slot_ids]
    heads_here = queries.shape[1] // HEAD
    query_blocks = queries.reshape(blocks_here, BLOCK, heads_here, HEAD)
    block_ids = device * blocks_here + jnp.arange(blocks_here, dtype=jnp.int32)
    scale = HEAD ** (-0.5)

    def attend(args):
        query_blk, picked, chosen, block_id, safe_row = args
        scores = (
            jnp.einsum(
                "qhd,nkd->hqnk", query_blk, picked[..., :HEAD], preferred_element_type=jnp.float32
            )
            * scale
        )
        query_pos = block_id * BLOCK + jnp.arange(BLOCK, dtype=jnp.int32)
        key_pos = safe_row[:, None] * BLOCK + jnp.arange(BLOCK, dtype=jnp.int32)[None, :]
        distance = query_pos[:, None, None] - key_pos[None, :, :]
        scores = scores - alibi_slope[:, None, None, None] * distance.astype(jnp.float32)[None]
        keep = (chosen >= 0)[None, :, None] & (distance >= 0)
        scores = jnp.where(keep[None], scores, -jnp.inf)
        weights = jax.nn.softmax(scores, axis=(2, 3)).astype(jnp.bfloat16)
        attended = jnp.einsum(
            "hqnk,nkd->qhd", weights, picked[..., HEAD:], preferred_element_type=jnp.float32
        )
        return attended.astype(jnp.bfloat16).reshape(BLOCK, heads_here * HEAD)

    attended = lax.map(attend, (query_blocks, selected, block_choice, block_ids, safe_ids))
    attended = attended.reshape(rows, heads_here * HEAD)
    result = jnp.dot(collect(attended, "tp", 1), out_weight, preferred_element_type=jnp.float32)
    return result.astype(jnp.bfloat16)


def solution(mesh):
    split = Mesh(mesh.devices.reshape(16, 4, 2, mesh.shape["tp"]), ("kv_0", "kv_1", "kv_2", "tp"))
    placed = (
        P(KV, None),
        P(None, "tp"),
        P(None, "tp"),
        P(None, "tp"),
        P(None, "tp"),
        P("tp"),
        P(KV, None),
    )
    return jax.shard_map(
        shards, mesh=split, in_specs=placed, out_specs=P(KV, "tp"), check_vma=False
    )
```

profile of v0, /device:TPU:32, one launch (start us, length us, event | category | flops | bytes accessed | tf_op | source)
XLA Modules:
  0.0 128.5 jit_solution(10849989266870693732)
XLA Ops:
  0.0 0.8 broadcast_maximum_fusion
  0.8 0.7 compare_and_fusion
  1.8 3.7 %all_to_all.20 = s32[64,2,1,1]{0,3,2,1:T(1,128)S(1)} all-to-all(s32[64,2,1,1]{0,3,2,1:T(1,128)S(1)} %copy.26), channel_id=1, replica_groups=mesh['kv_0'=16,'kv_1'=4,'kv_2'=2,'tp'=4] {'kv_2'}, dimensions={1} | all-to-all | bytes 1024 | tf_op jit(solution)/shard_map/all_to_all | solution.py:27
  5.5 0.7 copy.27
  6.2 18.2 %all-to-all-start.1 = ((s32[64,2,1,1]{1,3,2,0:T(1,128)}), s32[64,2,1,1]{1,3,2,0:T(1,128)S(1)}, u32[]{:S(2)}, u32[]{:S(2)}) async-start(s32[64,2,1,1]{1,3,2,0:T(1,128)} %copy.27), calls=%async_computation.1 | async-start | bytes 65536 | tf_op jit(solution)/shard_map/all_to_all | solution.py:27
  24.4 1.4 %convolution_convert_fusion.2 = bf16[128,64]{0,1:T(8,128)(2,1)S(1)} fusion(bf16[128,2048]{1,0:T(8,128)(2,1)} %param.9, bf16[2048,64]{0,1:T(8,128)(2,1)} %param.12), kind=kOutput, calls=%fused_computation.30 | convolution fusion | flops 33562624 | bytes 802816 | tf_op jit(solution)/shard_map/dot_general | solution.py:55
  25.8 1.4 %convolution_convert_fusion.3 = bf16[128,64]{0,1:T(8,128)(2,1)S(1)} fusion(bf16[128,2048]{1,0:T(8,128)(2,1)} %param.9, bf16[2048,64]{0,1:T(8,128)(2,1)} %param.11), kind=kOutput, calls=%fused_computation.31 | convolution fusion | flops 33562624 | bytes 802816 | tf_op jit(solution)/shard_map/dot_general | solution.py:54
  27.4 10.7 %all-to-all-done.1 = s32[64,2,1,1]{1,3,2,0:T(1,128)S(1)} async-done(((s32[64,2,1,1]{1,3,2,0:T(1,128)}), s32[64,2,1,1]{1,3,2,0:T(1,128)S(1)}, u32[]{:S(2)}, u32[]{:S(2)}) %all-to-all-start.1) | async-done | bytes 544 | tf_op jit(solution)/shard_map/all_to_all | solution.py:27
  38.4 1.7 %gather_fusion = bf16[128,32,128]{2,1,0:T(8,128)(2,1)} fusion(bf16[4,32,128]{2,1,0:T(8,128)(2,1)S(1)} %bitcast.76, s32[1024]{0:T(1024)S(1)} %pad_clamp_fusion.1), kind=kCustom, calls=%fused_computation | custom fusion | bytes 2097664 | tf_op jit(solution)/shard_map/gather | solution.py:65
  40.1 6.7 %all-to-all-start.2 = ((bf16[128,32,128]{2,1,0:T(8,128)(2,1)}), bf16[128,32,128]{2,1,0:T(8,128)(2,1)S(1)}, u32[]{:S(2)}, u32[]{:S(2)}) async-start(bf16[128,32,128]{2,1,0:T(8,128)(2,1)} %gather_fusion), calls=%async_computation.2 | async-start | bytes 2097152 | tf_op jit(solution)/shard_map/all_to_all | solution.py:66
  46.9 1.5 %convolution_convert_fusion.1 = bf16[128,256]{1,0:T(8,128)(2,1)S(1)} fusion(bf16[128,2048]{1,0:T(8,128)(2,1)S(1)} %copy-done.1, bf16[2048,256]{1,0:T(8,128)(2,1)} %param.10), kind=kOutput, calls=%fused_computation.29 | convolution fusion | flops 134250496 | bytes 1638400 | tf_op jit(solution)/shard_map/dot_general | solution.py:53
  48.6 53.4 %all-to-all-done.2 = bf16[128,32,128]{2,1,0:T(8,128)(2,1)S(1)} async-done(((bf16[128,32,128]{2,1,0:T(8,128)(2,1)}), bf16[128,32,128]{2,1,0:T(8,128)(2,1)S(1)}, u32[]{:S(2)}, u32[]{:S(2)}) %all-to-all-start.2) | async-done | bytes 1048608 | tf_op jit(solution)/shard_map/all_to_all | solution.py:66
  102.1 0.6 gather_fusion.1
  102.7 13.0 %while.10 = (s32[]{:T(128)}, bf16[4,32,256]{2,1,0:T(8,128)(2,1)S(1)}, bf16[4,8,32,128]{3,2,1,0:T(8,128)(2,1)S(1)}, s32[4,8]{1,0:T(4,128)}, s32[4]{0:T(128)S(1)},...) while((s32[]{:T(128)}, ...), condition=%wide.region_4.5_spmd, body=%wide.region_1.4_spmd.sunk | while | flops 8765491 | bytes 907445 | solution.py:95
  102.7 0.7 dynamic_slice.38
  104.2 0.7 compare_bitcast_fusion.2
  106.0 0.7 dynamic_slice.38
  107.5 0.7 compare_bitcast_fusion.2
  109.2 0.7 dynamic_slice.38
  110.7 0.7 compare_bitcast_fusion.2
  112.5 0.7 dynamic_slice.38
  114.0 0.7 compare_bitcast_fusion.2
  115.9 11.6 %all_to_all.21 = bf16[4,128,256]{1,2,0:T(8,128)(2,1)S(1)} all-to-all(bf16[4,128,256]{1,2,0:T(8,128)(2,1)S(1)} %broadcast_in_dim.61), channel_id=1, replica_groups=mesh['kv_0'=16,'kv_1'=4,'kv_2'=2,'tp'=4] {'tp'}, dimensions={0} | all-to-all | bytes 524288 | tf_op jit(solution)/shard_map/all_to_all | solution.py:39
  127.5 1.0 convolution_convert_fusion
  (75 shorter events, 5.7 us)
Async XLA Ops:
  0.0 127.5 %copy-start = (bf16[1024,512]{1,0:T(8,128)(2,1)S(1)}, bf16[1024,512]{1,0:T(8,128)(2,1)}, u32[]{:S(2)}) copy-start(bf16[1024,512]{1,0:T(8,128)(2,1)} %param.13) | copy-start | bytes 3145732
  6.2 31.9 %all-to-all-start.1 = ((s32[64,2,1,1]{1,3,2,0:T(1,128)}), s32[64,2,1,1]{1,3,2,0:T(1,128)S(1)}, u32[]{:S(2)}, u32[]{:S(2)}) async-start(s32[64,2,1,1]{1,3,2,0:T(1,128)} %copy.27), calls=%async_computation.1 | async-start | bytes 65536 | tf_op jit(solution)/shard_map/all_to_all | solution.py:27
  40.1 6.8 %copy-start.1 = (bf16[128,2048]{1,0:T(8,128)(2,1)S(1)}, bf16[128,2048]{1,0:T(8,128)(2,1)}, u32[]{:S(2)}) copy-start(bf16[128,2048]{1,0:T(8,128)(2,1)} %param.9) | copy-start | bytes 1572868
  40.1 61.9 %all-to-all-start.2 = ((bf16[128,32,128]{2,1,0:T(8,128)(2,1)}), bf16[128,32,128]{2,1,0:T(8,128)(2,1)S(1)}, u32[]{:S(2)}, u32[]{:S(2)}) async-start(bf16[128,32,128]{2,1,0:T(8,128)(2,1)} %gather_fusion), calls=%async_computation.2 | async-start | bytes 2097152 | tf_op jit(solution)/shard_map/all_to_all | solution.py:66
  48.6 54.2 %copy-start.2 = (f32[4]{0:T(128)S(1)}, f32[4]{0:T(128)}, u32[]{:S(2)}) copy-start(f32[4]{0:T(128)} %param.14) | copy-start | bytes 52
where the time goes:
time: 129 us
  waiting for transfers between devices  64.2 us (50%)
  starting transfers between devices  24.9 us (19%)
  blocking collectives  15.3 us (12%)
  matrix products  7.58 us (6%)
  local copies, waits for them, and re-layouts  7.12 us (6%)
  other arithmetic  6.2 us (5%)
  loops' own time  3.08 us (2%)
    all_to_all x1, waiting for transfers between devices, shards(): lax.all_to_all(outgoing, KV, split_axis=0, concat_axis=0, tiled=True)  53.4 us
    all_to_all x1, starting transfers between devices, exchange_in_order(): lax.all_to_all(tiles, axes[k], split_axis=k, concat_axis=k, tiled=True)  18.2 us
    all_to_all x1, blocking collectives, copy_for_each(): lax.all_to_all(jnp.broadcast_to(value[None], (peers, *value.shape)), axis...  11.6 us
    all_to_all x1, waiting for transfers between devices, exchange_in_order(): lax.all_to_all(tiles, axes[k], split_axis=k, concat_axis=k, tiled=True)  10.7 us
    all_to_all x1, starting transfers between devices, shards(): lax.all_to_all(outgoing, KV, split_axis=0, concat_axis=0, tiled=True)  6.68 us
    all_to_all x1, blocking collectives, exchange_in_order(): lax.all_to_all(tiles, axes[k], split_axis=k, concat_axis=k, tiled=True)  3.7 us
    another operation x1, loops' own time, shards(): lax.map(attend, (query_blocks, selected, block_choice, block_ids, safe_ids))  3.08 us
    ge x4, other arithmetic, attend(): keep = (chosen >= 0)[None, :, None] & (distance >= 0)  2.76 us
  transfers between devices with their start and end apart: 2, of which 2 were waited for; matrix products, arithmetic and copies ran while one was open for 4% of the time, Pallas kernels for 0%

commit v1 on v0

v1 whole, which is shorter than its diff:
```python
import functools

import jax
import jax.numpy as jnp
from jax import lax
from jax.experimental import pallas as pl
from jax.experimental.pallas import tpu as pltpu
from jax.sharding import Mesh
from jax.sharding import PartitionSpec as P

HEAD = 64
BLOCK = 32
KV = ("z_far", "z_near", "x", "core")
GATHERED = ("z_far", "core")
SELECTED = ("z_near", "x")
FAR_POSITION = 1 << 20

VMEM = pl.BlockSpec(memory_space=pltpu.VMEM)
SMEM = pl.BlockSpec(memory_space=pltpu.SMEM)
GRANT = pltpu.CompilerParams(vmem_limit_bytes=12 << 20)


def wanted_kernel(columns, cores, choice_ref, wanted_ref):
    blocks_here, topk = choice_ref.shape
    shape = wanted_ref.shape
    column = lax.broadcasted_iota(jnp.int32, shape, 0)
    member = lax.broadcasted_iota(jnp.int32, shape, 2)
    owner = (member // cores) * (columns * cores) + column * cores + member % cores
    wanted = jnp.full(shape, -1, jnp.int32)
    for g in range(blocks_here):
        for n in range(1, topk):
            chosen = choice_ref[g, n]
            named = jnp.where(chosen >= 0, chosen // blocks_here, -1)
            wanted = jnp.where(owner == named, chosen % blocks_here, wanted)
    wanted_ref[...] = wanted


def project_kernel(tokens_ref, key_ref, value_ref, packed_ref):
    weights = jnp.concatenate([key_ref[...], value_ref[...]], axis=0)
    packed = lax.dot_general(
        tokens_ref[...], weights, (((1,), (1,)), ((), ())), preferred_element_type=jnp.float32
    )
    packed_ref[...] = packed.astype(packed_ref.dtype)


def select_kernel(blocks_here, asked_ref, gathered_ref, outgoing_ref):
    columns, members = outgoing_ref.shape[:2]

    @pl.loop(0, columns)
    def _(column):
        for member in range(members):
            local = jnp.maximum(asked_ref[column, 0, member], 0)
            outgoing_ref[column, member] = gathered_ref[member * blocks_here + local]


def attend_kernel(columns, cores, choice_ref, slope_ref, queries_ref, own_ref, incoming_ref, out_ref):
    blocks_here, topk = choice_ref.shape
    members = incoming_ref.shape[0] // columns
    heads = queries_ref.shape[1] // HEAD
    keys = topk * BLOCK
    device = choice_ref[0, 0] // blocks_here
    lane = lax.broadcasted_iota(jnp.int32, (BLOCK, 2 * HEAD), 1)
    query_row = lax.broadcasted_iota(jnp.int32, (BLOCK, keys), 0)
    key_lane = lax.broadcasted_iota(jnp.int32, (1, keys), 1)
    for g in range(blocks_here):
        picked = []
        key_pos = jnp.zeros((1, keys), jnp.int32)
        for n in range(topk):
            chosen = choice_ref[g, n]
            safe = jnp.maximum(chosen, 0)
            owner = safe // blocks_here
            local = safe % blocks_here
            column = (owner // cores) % columns
            member = owner // (columns * cores) * cores + owner % cores
            block = jnp.where(owner == device, own_ref[local], incoming_ref[column * members + member])
            picked.append(block)
            first = jnp.where(chosen >= 0, chosen * BLOCK, FAR_POSITION)
            key_pos = jnp.where(key_lane // BLOCK == n, first, key_pos)
        table = jnp.concatenate(picked, axis=0)
        key_pos = key_pos + key_lane % BLOCK
        query_pos = (device * blocks_here + g) * BLOCK + query_row
        distance = query_pos - key_pos
        keep = distance >= 0
        far = distance.astype(jnp.float32)
        rows = pl.ds(g * BLOCK, BLOCK)
        padded = []
        for h in range(heads):
            pair = queries_ref[rows, pl.ds(h // 2 * 2 * HEAD, 2 * HEAD)].astype(jnp.float32)
            if h % 2:
                pair = pltpu.roll(pair, HEAD, 1)
            padded.append(jnp.where(lane < HEAD, pair, 0.0).astype(jnp.bfloat16))
        query = jnp.concatenate(padded, axis=0)
        raw = lax.dot_general(
            query, table, (((1,), (1,)), ((), ())), preferred_element_type=jnp.float32
        )
        weights = []
        for h in range(heads):
            scores = raw[h * BLOCK : (h + 1) * BLOCK] * (HEAD**-0.5) - slope_ref[h] * far
            scores = jnp.where(keep, scores, -jnp.inf)
            top = jnp.max(scores, axis=1, keepdims=True)
            expd = jnp.exp(scores - top)
            total = jnp.sum(expd, axis=1, keepdims=True)
            weights.append((expd / total).astype(jnp.bfloat16))
        summed = jnp.dot(
            jnp.concatenate(weights, axis=0), table, preferred_element_type=jnp.float32
        )
        for h in range(0, heads, 2):
            even = pltpu.roll(summed[h * BLOCK : (h + 1) * BLOCK], HEAD, 1)
            odd = summed[(h + 1) * BLOCK : (h + 2) * BLOCK]
            out_ref[rows, pl.ds(h * HEAD, 2 * HEAD)] = jnp.where(lane < HEAD, even, odd).astype(
                out_ref.dtype
            )


def shards(tokens, query_weight, key_weight, value_weight, out_weight, alibi_slope, block_choice):
    rows = tokens.shape[0]
    blocks_here = rows // BLOCK
    columns = lax.axis_size(SELECTED)
    cores = lax.axis_size("core")
    members = lax.axis_size(GATHERED)
    wanted = pl.pallas_call(
        functools.partial(wanted_kernel, columns, cores),
        out_shape=jax.ShapeDtypeStruct((columns, 1, 128), jnp.int32),
        in_specs=[SMEM],
        out_specs=VMEM,
        name="wanted",
        compiler_params=GRANT,
    )(block_choice)
    asked = lax.all_to_all(wanted, SELECTED, 0, 0, tiled=True)
    packed = pl.pallas_call(
        project_kernel,
        out_shape=jax.ShapeDtypeStruct((rows, 2 * HEAD), jnp.bfloat16),
        in_specs=[VMEM] * 3,
        out_specs=VMEM,
        name="project",
        compiler_params=GRANT,
        cost_estimate=pl.CostEstimate(
            flops=2 * rows * tokens.shape[1] * 2 * HEAD, bytes_accessed=1 << 20, transcendentals=0
        ),
    )(tokens, key_weight.T, value_weight.T)
    gathered = lax.all_gather(packed, GATHERED, axis=0, tiled=True)
    outgoing = pl.pallas_call(
        functools.partial(select_kernel, blocks_here),
        out_shape=jax.ShapeDtypeStruct((columns, members, BLOCK, 2 * HEAD), jnp.bfloat16),
        in_specs=[SMEM, VMEM],
        out_specs=VMEM,
        name="select",
        compiler_params=GRANT,
    )(asked, gathered.reshape(members * blocks_here, BLOCK, 2 * HEAD))
    incoming = lax.all_to_all(outgoing, SELECTED, 0, 0, tiled=True)
    queries = jnp.dot(tokens, query_weight, preferred_element_type=jnp.float32).astype(jnp.bfloat16)
    attended = pl.pallas_call(
        functools.partial(attend_kernel, columns, cores),
        out_shape=jax.ShapeDtypeStruct(queries.shape, jnp.bfloat16),
        in_specs=[SMEM, SMEM, VMEM, VMEM, VMEM],
        out_specs=VMEM,
        name="attend",
        compiler_params=GRANT,
    )(
        block_choice,
        alibi_slope,
        queries,
        packed.reshape(blocks_here, BLOCK, 2 * HEAD),
        incoming.reshape(columns * members, BLOCK, 2 * HEAD),
    )
    peers = lax.axis_size("tp")
    everyone = lax.all_to_all(
        jnp.broadcast_to(attended[None], (peers, *attended.shape)), "tp", 0, 0, tiled=True
    )
    everyone = jnp.moveaxis(everyone, 0, 1).reshape(rows, -1)
    result = jnp.dot(everyone, out_weight, preferred_element_type=jnp.float32)
    return result.astype(jnp.bfloat16)


def solution(mesh):
    split = Mesh(
        mesh.devices.reshape(8, 2, 4, 2, mesh.shape["tp"]), ("z_far", "z_near", "x", "core", "tp")
    )
    placed = (
        P(KV, None),
        P(None, "tp"),
        P(None, "tp"),
        P(None, "tp"),
        P(None, "tp"),
        P("tp"),
        P(KV, None),
    )
    return jax.shard_map(
        shards, mesh=split, in_specs=placed, out_specs=P(KV, "tp"), check_vma=False
    )
```

time: 129 us -> 75.9 us (0.59)
  waiting for transfers between devices: 64.2 us -> 13.2 us
  blocking collectives: 15.3 us -> 34.9 us
  starting transfers between devices: 24.9 us -> 15 us
  other arithmetic: 6.2 us -> 0 us
  Pallas kernels: 0 us -> 5.28 us
  matrix products: 7.58 us -> 2.54 us
  loops' own time: 3.08 us -> 0 us
  local copies, waits for them, and re-layouts: 7.12 us -> 4.53 us
    all_to_all x2, waiting for transfers between devices: 64.2 us -> 13.2 us  [the longest x1 13.2 us: shards(): incoming = lax.all_to_all(outgoing, SELECTED, 0, 0, tiled=True)]
    all_gather x0 -> x1, blocking collectives: none -> 23.9 us  [shards(): gathered = lax.all_gather(packed, GATHERED, axis=0, tiled=True)]
    all_to_all x2, starting transfers between devices: 24.9 us -> 15 us  [the longest x1 8.69 us: shards(): asked = lax.all_to_all(wanted, SELECTED, 0, 0, tiled=True)]
    pallas_call x0 -> x4, Pallas kernels: none -> 5.28 us  [the longest x1 1.84 us: shards(): pl.pallas_call(functools.partial(attend_kernel, columns, cores), out_shap...]
    dot_general x11 -> x1, matrix products: 6.05 us -> 1.01 us  [shards(): result = jnp.dot(everyone, out_weight, preferred_element_type=jnp.float32)]
    all_to_all x2 -> x1, blocking collectives: 15.3 us -> 10.9 us  [shards(): lax.all_to_all(jnp.broadcast_to(attended[None], (peers, *attended.shape))...]
    unnamed x6 -> x16, local copies, waits for them, and re-layouts: 0.01 us -> 4.38 us
    another operation x1 -> x0, loops' own time: 3.08 us -> none  [shards(): lax.map(attend, (query_blocks, selected, block_choice, block_ids, safe_ids))]
  transfers between devices with their start and end apart: 2 -> 2, of which waited for: 2 -> 1; matrix products, arithmetic and copies ran while one was open for 4% -> 2% of each run, Pallas kernels for 0% -> 0%
where the time goes in v1:
time: 75.9 us; the launch traced here: 75.5 us
  blocking collectives  34.9 us (46%)
  starting transfers between devices  15 us (20%)
  waiting for transfers between devices  13.2 us (17%)
  Pallas kernels  5.28 us (7%)
  local copies, waits for them, and re-layouts  4.53 us (6%)
  matrix products  2.54 us (3%)
    all_gather x1, blocking collectives, shards(): gathered = lax.all_gather(packed, GATHERED, axis=0, tiled=True)  23.9 us
    all_to_all x1, waiting for transfers between devices, shards(): incoming = lax.all_to_all(outgoing, SELECTED, 0, 0, tiled=True)  13.2 us
    all_to_all x1, blocking collectives, shards(): lax.all_to_all(jnp.broadcast_to(attended[None], (peers, *attended.shape))...  10.9 us
    all_to_all x1, starting transfers between devices, shards(): asked = lax.all_to_all(wanted, SELECTED, 0, 0, tiled=True)  8.69 us
    all_to_all x1, starting transfers between devices, shards(): incoming = lax.all_to_all(outgoing, SELECTED, 0, 0, tiled=True)  6.3 us
    unnamed x16, local copies, waits for them, and re-layouts  4.38 us
    pallas_call x1, Pallas kernels, shards(): pl.pallas_call(functools.partial(attend_kernel, columns, cores), out_shap...  1.84 us
    pallas_call x1, Pallas kernels, shards(): pl.pallas_call(functools.partial(select_kernel, blocks_here), out_shape=j...  1.81 us
  transfers between devices with their start and end apart: 2, of which 1 were waited for; matrix products, arithmetic and copies ran while one was open for 2% of the time, Pallas kernels for 0%

profile of v1, /device:TPU:32, one launch (start us, length us, event | category | flops | bytes accessed | tf_op | source)
XLA Modules:
  0.0 75.5 jit_solution(11863237322269702251)
XLA Ops:
  0.0 0.0 copy-start
  0.0 0.0 copy-start.5
  0.0 0.8 %copy-done.5 = s32[4,8]{1,0:T(4,128)S(1)} copy-done((s32[4,8]{1,0:T(4,128)S(1)}, s32[4,8]{1,0:T(4,128)}, u32[]{:S(2)}) %copy-start.5) | copy-done | bytes 152
  0.8 1.3 %wanted.1 = s32[8,1,128]{2,1,0:T(1,128)} custom-call(s32[4,8]{1,0:T(4,128)S(1)} %copy-done.5), custom_call_target="tpu_custom_call" | custom-call | tf_op jit(solution)/shard_map/wanted/pallas_call | solution.py:121
  2.1 8.7 %all-to-all-start = ((s32[8,1,128]{2,1,0:T(1,128)}), s32[8,1,128]{2,1,0:T(1,128)S(1)}, u32[]{:S(2)}, u32[]{:S(2)}) async-start(s32[8,1,128]{2,1,0:T(1,128)} %wanted.1), calls=%async_computation | async-start | bytes 8192 | tf_op jit(solution)/shard_map/all_to_all | solution.py:129
  10.8 1.0 %copy-done.1 = bf16[128,2048]{1,0:T(8,128)(2,1)S(1)} copy-done((bf16[128,2048]{1,0:T(8,128)(2,1)S(1)}, bf16[128,2048]{1,0:T(8,128)(2,1)}, u32[]{:S(2)}) %copy-start.1) | copy-done | bytes 524312
  11.8 0.9 %copy-done.3 = bf16[2048,64]{0,1:T(8,128)(2,1)S(1)} copy-done((bf16[2048,64]{0,1:T(8,128)(2,1)S(1)}, bf16[2048,64]{0,1:T(8,128)(2,1)}, u32[]{:S(2)}) %copy-start.3) | copy-done | bytes 262168
  12.8 0.9 %copy-done.4 = bf16[2048,64]{0,1:T(8,128)(2,1)S(1)} copy-done((bf16[2048,64]{0,1:T(8,128)(2,1)S(1)}, bf16[2048,64]{0,1:T(8,128)(2,1)}, u32[]{:S(2)}) %copy-start.4) | copy-done | bytes 262168
  13.7 0.3 project.1
  14.0 23.9 %all_gather.3 = bf16[2048,128]{1,0:T(8,128)(2,1)S(1)} all-gather(bf16[128,128]{1,0:T(8,128)(2,1)S(1)} %project.1), channel_id=1, replica_groups=mesh['z_far'=8,'z_near'=2,'x'=4,'core'=2,'tp'=4] {'z_far','core'}, dimensions={0}, use_global_device_ids=true | all-gather | bytes 557056 | tf_op jit(solution)/shard_map/all_gather | solution.py:141
  38.0 0.0 all-to-all-done.asked_ref
  38.0 1.8 %select.1 = bf16[8,16,32,128]{3,2,1,0:T(8,128)(2,1)} custom-call(s32[8,1,128]{2,1,0:T(1,128)S(1)} %all-to-all-done.asked_ref, bf16[64,32,128]{2,1,0:T(8,128)(2,1)S(1)} %bitcast.13), custom_call_target="tpu_custom_call" | custom-call | tf_op jit(solution)/shard_map/select/pallas_call | solution.py:142
  39.8 6.3 %all-to-all-start.1 = ((bf16[8,16,32,128]{3,2,1,0:T(8,128)(2,1)}), bf16[8,16,32,128]{3,2,1,0:T(8,128)(2,1)S(1)}, u32[]{:S(2)}, u32[]{:S(2)}) async-start(bf16[8,16,32,128]{3,2,1,0:T(8,128)(2,1)} %select.1), calls=%async_computation.1 | async-start | bytes 2097152 | tf_op jit(solution)/shard_map/all_to_all | solution.py:150
  46.1 0.0 copy-done.2
  46.1 1.5 %convolution_convert_fusion.1.queries_ref = bf16[128,256]{1,0:T(8,128)(2,1)S(1)} fusion(bf16[128,2048]{1,0:T(8,128)(2,1)S(1)} %copy-done.2, bf16[2048,256]{1,0:T(8,128)(2,1)} %param.8), kind=kOutput, calls=%fused_computation.1 | convolution fusion | flops 134250496 | bytes 1638400 | tf_op jit(solution)/shard_map/dot_general | solution.py:151
  47.6 0.0 copy-start.6
  47.6 13.2 %all-to-all-done.1 = bf16[8,16,32,128]{3,2,1,0:T(8,128)(2,1)S(1)} async-done(((bf16[8,16,32,128]{3,2,1,0:T(8,128)(2,1)}), bf16[8,16,32,128]{3,2,1,0:T(8,128)(2,1)S(1)}, u32[]{:S(2)}, u32[]{:S(2)}) %all-to-all-start.1) | async-done | bytes 1048608 | tf_op jit(solution)/shard_map/all_to_all | solution.py:150
  60.8 0.0 copy-done.6
  60.8 0.7 copy-done.7
  61.5 1.8 %attend.1 = bf16[128,256]{1,0:T(8,128)(2,1)S(1)} custom-call(s32[4,8]{1,0:T(4,128)S(1)} %copy-done.6, f32[4]{0:T(128)S(1)} %copy-done.7, bf16[128,256]{1,0:T(8,128)(2,1)S(1)} %convolution_convert_fusion.1.queries_ref, bf16[4,32,128]{2,1,0:T(8,128)(2,1)S(1)} %bitcast.14, bf16[128,32,128]{2,1,0:T(8,128)(2,1)S(1)} %bitcast.12), custom_call_target="tpu_custom_call" | custom-call | tf_op jit(solution)/shard_map/attend/pallas_call | solution.py:152
  63.3 0.1 copy.8
  63.5 10.9 %all_to_all.15 = bf16[4,128,256]{1,2,0:T(8,128)(2,1)S(1)} all-to-all(bf16[4,128,256]{1,2,0:T(8,128)(2,1)S(1)} %broadcast_in_dim.2), channel_id=1, replica_groups=mesh['z_far'=8,'z_near'=2,'x'=4,'core'=2,'tp'=4] {'tp'}, dimensions={0} | all-to-all | bytes 524288 | tf_op jit(solution)/shard_map/all_to_all | solution.py:167
  74.4 0.0 copy-done
  74.4 1.0 %convolution_convert_fusion = bf16[128,512]{1,0:T(8,128)(2,1)} fusion(bf16[128,1024]{0,1:T(8,128)(2,1)S(1)} %bitcast.17, bf16[1024,512]{1,0:T(8,128)(2,1)S(1)} %copy-done), kind=kOutput, calls=%fused_computation | convolution fusion | flops 134283264 | bytes 1441792 | tf_op jit(solution)/shard_map/dot_general | solution.py:171
  (6 shorter events, 0.0 us)
Async XLA Ops:
  0.0 74.4 %copy-start = (bf16[1024,512]{1,0:T(8,128)(2,1)S(1)}, bf16[1024,512]{1,0:T(8,128)(2,1)}, u32[]{:S(2)}) copy-start(bf16[1024,512]{1,0:T(8,128)(2,1)} %param.11) | copy-start | bytes 3145732
  0.0 0.8 %copy-start.5 = (s32[4,8]{1,0:T(4,128)S(1)}, s32[4,8]{1,0:T(4,128)}, u32[]{:S(2)}) copy-start(s32[4,8]{1,0:T(4,128)} %choice_ref.3) | copy-start | bytes 388
  2.1 35.9 %all-to-all-start = ((s32[8,1,128]{2,1,0:T(1,128)}), s32[8,1,128]{2,1,0:T(1,128)S(1)}, u32[]{:S(2)}, u32[]{:S(2)}) async-start(s32[8,1,128]{2,1,0:T(1,128)} %wanted.1), calls=%async_computation | async-start | bytes 8192 | tf_op jit(solution)/shard_map/all_to_all | solution.py:129
  10.8 1.0 %copy-start.1 = (bf16[128,2048]{1,0:T(8,128)(2,1)S(1)}, bf16[128,2048]{1,0:T(8,128)(2,1)}, u32[]{:S(2)}) copy-start(bf16[128,2048]{1,0:T(8,128)(2,1)} %tokens_ref.1) | copy-start | bytes 1572868
  11.8 0.9 %copy-start.3 = (bf16[2048,64]{0,1:T(8,128)(2,1)S(1)}, bf16[2048,64]{0,1:T(8,128)(2,1)}, u32[]{:S(2)}) copy-start(bf16[2048,64]{0,1:T(8,128)(2,1)} %param.9) | copy-start | bytes 786436
  12.8 0.9 %copy-start.4 = (bf16[2048,64]{0,1:T(8,128)(2,1)S(1)}, bf16[2048,64]{0,1:T(8,128)(2,1)}, u32[]{:S(2)}) copy-start(bf16[2048,64]{0,1:T(8,128)(2,1)} %param.10) | copy-start | bytes 786436
  39.8 6.3 %copy-start.2 = (bf16[128,2048]{1,0:T(8,128)(2,1)S(1)}, bf16[128,2048]{1,0:T(8,128)(2,1)}, u32[]{:S(2)}) copy-start(bf16[128,2048]{1,0:T(8,128)(2,1)} %tokens_ref.1) | copy-start | bytes 1572868
  39.8 21.1 %all-to-all-start.1 = ((bf16[8,16,32,128]{3,2,1,0:T(8,128)(2,1)}), bf16[8,16,32,128]{3,2,1,0:T(8,128)(2,1)S(1)}, u32[]{:S(2)}, u32[]{:S(2)}) async-start(bf16[8,16,32,128]{3,2,1,0:T(8,128)(2,1)} %select.1), calls=%async_computation.1 | async-start | bytes 2097152 | tf_op jit(solution)/shard_map/all_to_all | solution.py:150
  47.6 13.2 %copy-start.6 = (s32[4,8]{1,0:T(4,128)S(1)}, s32[4,8]{1,0:T(4,128)}, u32[]{:S(2)}) copy-start(s32[4,8]{1,0:T(4,128)} %choice_ref.3) | copy-start | bytes 388
  60.8 0.7 copy-start.7

commit v2 on v1

--- a/solution.py
+++ b/solution.py
@@ -16,11 +16,47 @@
 FAR_POSITION = 1 << 20
 
 VMEM = pl.BlockSpec(memory_space=pltpu.VMEM)
+HBM = pl.BlockSpec(memory_space=pltpu.HBM)
 SMEM = pl.BlockSpec(memory_space=pltpu.SMEM)
 GRANT = pltpu.CompilerParams(vmem_limit_bytes=12 << 20)
 
 
-def wanted_kernel(columns, cores, choice_ref, wanted_ref):
+def in_hbm(value):
+    return pltpu.with_memory_space_constraint(value, pltpu.HBM)
+
+
+def prepare_kernel(
+    columns,
+    cores,
+    choice_hbm,
+    tokens_hbm,
+    key_hbm,
+    value_hbm,
+    query_hbm,
+    slope_hbm,
+    wanted_ref,
+    packed_ref,
+    queries_ref,
+    near_choice_ref,
+    near_slope_ref,
+    choice_ref,
+    tokens_ref,
+    packed_weight_ref,
+    query_weight_ref,
+    sems,
+):
+    copies = [
+        pltpu.make_async_copy(choice_hbm, choice_ref, sems.at[0]),
+        pltpu.make_async_copy(tokens_hbm, tokens_ref, sems.at[1]),
+        pltpu.make_async_copy(key_hbm, packed_weight_ref.at[pl.ds(0, HEAD)], sems.at[2]),
+        pltpu.make_async_copy(value_hbm, packed_weight_ref.at[pl.ds(HEAD, HEAD)], sems.at[3]),
+        pltpu.make_async_copy(query_hbm, query_weight_ref, sems.at[4]),
+        pltpu.make_async_copy(choice_hbm, near_choice_ref, sems.at[5]),
+        pltpu.make_async_copy(slope_hbm, near_slope_ref, sems.at[6]),
+    ]
+    for copy in copies:
+        copy.start()
+    copies[0].wait()
     blocks_here, topk = choice_ref.shape
     shape = wanted_ref.shape
     column = lax.broadcasted_iota(jnp.int32, shape, 0)
@@ -33,14 +69,19 @@
             named = jnp.where(chosen >= 0, chosen // blocks_here, -1)
             wanted = jnp.where(owner == named, chosen % blocks_here, wanted)
     wanted_ref[...] = wanted
-
-
-def project_kernel(tokens_ref, key_ref, value_ref, packed_ref):
-    weights = jnp.concatenate([key_ref[...], value_ref[...]], axis=0)
+    for copy in copies[1:4]:
+        copy.wait()
     packed = lax.dot_general(
-        tokens_ref[...], weights, (((1,), (1,)), ((), ())), preferred_element_type=jnp.float32
+        tokens_ref[...],
+        packed_weight_ref[...],
+        (((1,), (1,)), ((), ())),
+        preferred_element_type=jnp.float32,
     )
     packed_ref[...] = packed.astype(packed_ref.dtype)
+    for copy in copies[4:]:
+        copy.wait()
+    queries = jnp.dot(tokens_ref[...], query_weight_ref[...], preferred_element_type=jnp.float32)
+    queries_ref[...] = queries.astype(queries_ref.dtype)
 
 
 def select_kernel(blocks_here, asked_ref, gathered_ref, outgoing_ref):
@@ -118,26 +159,35 @@
     columns = lax.axis_size(SELECTED)
     cores = lax.axis_size("core")
     members = lax.axis_size(GATHERED)
-    wanted = pl.pallas_call(
-        functools.partial(wanted_kernel, columns, cores),
-        out_shape=jax.ShapeDtypeStruct((columns, 1, 128), jnp.int32),
-        in_specs=[SMEM],
-        out_specs=VMEM,
-        name="wanted",
+    wanted, packed, queries, choice, slope = pl.pallas_call(
+        functools.partial(prepare_kernel, columns, cores),
+        out_shape=(
+            jax.ShapeDtypeStruct((columns, 1, 128), jnp.int32),
+            jax.ShapeDtypeStruct((rows, 2 * HEAD), jnp.bfloat16),
+            jax.ShapeDtypeStruct((rows, query_weight.shape[1]), jnp.bfloat16),
+            jax.ShapeDtypeStruct(block_choice.shape, jnp.int32),
+            jax.ShapeDtypeStruct(alibi_slope.shape, jnp.float32),
+        ),
+        in_specs=[HBM] * 6,
+        out_specs=(VMEM,) * 5,
+        scratch_shapes=[
+            pltpu.SMEM(block_choice.shape, jnp.int32),
+            pltpu.VMEM(tokens.shape, jnp.bfloat16),
+            pltpu.VMEM((2 * HEAD, tokens.shape[1]), jnp.bfloat16),
+            pltpu.VMEM(query_weight.shape, jnp.bfloat16),
+            pltpu.SemaphoreType.DMA((7,)),
+        ],
+        name="prepare",
         compiler_params=GRANT,
-    )(block_choice)
+    )(
+        in_hbm(block_choice),
+        in_hbm(tokens),
+        in_hbm(key_weight.T),
+        in_hbm(value_weight.T),
+        in_hbm(query_weight),
+        in_hbm(alibi_slope),
+    )
     asked = lax.all_to_all(wanted, SELECTED, 0, 0, tiled=True)
-    packed = pl.pallas_call(
-        project_kernel,
-        out_shape=jax.ShapeDtypeStruct((rows, 2 * HEAD), jnp.bfloat16),
-        in_specs=[VMEM] * 3,
-        out_specs=VMEM,
-        name="project",
-        compiler_params=GRANT,
-        cost_estimate=pl.CostEstimate(
-            flops=2 * rows * tokens.shape[1] * 2 * HEAD, bytes_accessed=1 << 20, transcendentals=0
-        ),
-    )(tokens, key_weight.T, value_weight.T)
     gathered = lax.all_gather(packed, GATHERED, axis=0, tiled=True)
     outgoing = pl.pallas_call(
         functools.partial(select_kernel, blocks_here),
@@ -148,7 +198,6 @@
         compiler_params=GRANT,
     )(asked, gathered.reshape(members * blocks_here, BLOCK, 2 * HEAD))
     incoming = lax.all_to_all(outgoing, SELECTED, 0, 0, tiled=True)
-    queries = jnp.dot(tokens, query_weight, preferred_element_type=jnp.float32).astype(jnp.bfloat16)
     attended = pl.pallas_call(
         functools.partial(attend_kernel, columns, cores),
         out_shape=jax.ShapeDtypeStruct(queries.shape, jnp.bfloat16),
@@ -157,8 +206,8 @@
         name="attend",
         compiler_params=GRANT,
     )(
-        block_choice,
-        alibi_slope,
+        choice,
+        slope,
         queries,
         packed.reshape(blocks_here, BLOCK, 2 * HEAD),
         incoming.reshape(columns * members, BLOCK, 2 * HEAD),

time: 75.9 us -> 71 us (0.935)
  the two profiles are of different devices: /device:TPU:32 before, /device:TPU:8 now
where the time goes in v2:
time: 71 us; the launch traced here: 70.7 us
  blocking collectives  58.8 us (83%)
  starting transfers between devices  5.67 us (8%)
  Pallas kernels  5.05 us (7%)
  matrix products  1.01 us (1%)
    all_gather x1, blocking collectives, shards(): gathered = lax.all_gather(packed, GATHERED, axis=0, tiled=True)  26.5 us
    all_to_all x1, blocking collectives, shards(): incoming = lax.all_to_all(outgoing, SELECTED, 0, 0, tiled=True)  22.3 us
    all_to_all x1, blocking collectives, shards(): lax.all_to_all(jnp.broadcast_to(attended[None], (peers, *attended.shape))...  9.93 us
    all_to_all x1, starting transfers between devices, shards(): asked = lax.all_to_all(wanted, SELECTED, 0, 0, tiled=True)  5.67 us
    pallas_call x1, Pallas kernels, shards(): pl.pallas_call(functools.partial(prepare_kernel, columns, cores), out_sha...  2.36 us
    pallas_call x1, Pallas kernels, shards(): pl.pallas_call(functools.partial(attend_kernel, columns, cores), out_shap...  1.84 us
  transfers between devices with their start and end apart: 1, of which 0 were waited for; matrix products, arithmetic and copies ran while one was open for 0% of the time, Pallas kernels for 0%

profile of v2, /device:TPU:8, one launch (start us, length us, event | category | flops | bytes accessed | tf_op | source)
XLA Modules:
  0.0 70.7 jit_solution(3133792147609296682)
XLA Ops:
  0.0 0.0 copy-start
  0.0 2.4 %prepare.1 = (s32[8,1,128]{2,1,0:T(1,128)}, bf16[128,128]{1,0:T(8,128)(2,1)S(1)}, bf16[128,256]{1,0:T(8,128)(2,1)S(1)}, s32[4,8]{1,0:T(4,128)S(1)}, f32[4]{0:T(128)S(1)}) custom-call(s32[4,8]{1,0:T(4,128)} %choice_hbm.1, bf16[128,2048]{1,0:T(8,128)(2,1)} %tokens_hbm.1, bf16[64,2048]{1,0:T(8,128)(2,1)} %bitcast.14, bf16[64,2048]{1,0:T(8,128)(2,1)} %bitcast.15, ...), custom_call_target="tpu_custom_call" | custom-call | tf_op jit(solution)/shard_map/prepare/pallas_call | solution.py:162
  2.4 5.7 %all-to-all-start = ((s32[8,1,128]{2,1,0:T(1,128)}), s32[8,1,128]{2,1,0:T(1,128)S(1)}, u32[]{:S(2)}, u32[]{:S(2)}) async-start(s32[8,1,128]{2,1,0:T(1,128)} %get-tuple-element.14), calls=%async_computation | async-start | bytes 8192 | tf_op jit(solution)/shard_map/all_to_all | solution.py:190
  8.0 26.5 %all_gather.3 = bf16[2048,128]{1,0:T(8,128)(2,1)S(1)} all-gather(bf16[128,128]{1,0:T(8,128)(2,1)S(1)} %get-tuple-element.13), channel_id=1, replica_groups=mesh['z_far'=8,'z_near'=2,'x'=4,'core'=2,'tp'=4] {'z_far','core'}, dimensions={0}, use_global_device_ids=true | all-gather | bytes 557056 | tf_op jit(solution)/shard_map/all_gather | solution.py:191
  34.6 0.0 all-to-all-done.asked_ref
  34.6 0.8 %select.1 = bf16[8,16,32,128]{3,2,1,0:T(8,128)(2,1)S(1)} custom-call(s32[8,1,128]{2,1,0:T(1,128)S(1)} %all-to-all-done.asked_ref, bf16[64,32,128]{2,1,0:T(8,128)(2,1)S(1)} %bitcast.11), custom_call_target="tpu_custom_call" | custom-call | tf_op jit(solution)/shard_map/select/pallas_call | solution.py:192
  35.4 22.3 %all_to_all.15 = bf16[8,16,32,128]{3,2,1,0:T(8,128)(2,1)S(1)} all-to-all(bf16[8,16,32,128]{3,2,1,0:T(8,128)(2,1)S(1)} %select.1), channel_id=1, replica_groups=mesh['z_far'=8,'z_near'=2,'x'=4,'core'=2,'tp'=4] {'z_near','x'}, dimensions={0} | all-to-all | bytes 2097152 | tf_op jit(solution)/shard_map/all_to_all | solution.py:200
  57.8 1.8 %attend.1 = bf16[128,256]{1,0:T(8,128)(2,1)S(1)} custom-call(s32[4,8]{1,0:T(4,128)S(1)} %get-tuple-element.10.choice_ref, f32[4]{0:T(128)S(1)} %get-tuple-element.11.slope_ref, bf16[128,256]{1,0:T(8,128)(2,1)S(1)} %get-tuple-element.12.queries_ref, bf16[4,32,128]{2,1,0:T(8,128)(2,1)S(1)} %bitcast.12, bf16[128,32,128]{2,1,0:T(8,128)(2,1)S(1)} %bitcast.10), custom_call_target="tpu_custom_call" | custom-call | tf_op jit(solution)/shard_map/attend/pallas_call | solution.py:201
  59.6 0.1 copy.8
  59.8 9.9 %all_to_all.16 = bf16[4,128,256]{1,2,0:T(8,128)(2,1)S(1)} all-to-all(bf16[4,128,256]{1,2,0:T(8,128)(2,1)S(1)} %broadcast_in_dim.2), channel_id=1, replica_groups=mesh['z_far'=8,'z_near'=2,'x'=4,'core'=2,'tp'=4] {'tp'}, dimensions={0} | all-to-all | bytes 524288 | tf_op jit(solution)/shard_map/all_to_all | solution.py:216
  69.7 0.0 copy-done
  69.7 1.0 %convolution_convert_fusion = bf16[128,512]{1,0:T(8,128)(2,1)} fusion(bf16[128,1024]{0,1:T(8,128)(2,1)S(1)} %bitcast.13, bf16[1024,512]{1,0:T(8,128)(2,1)S(1)} %copy-done), kind=kOutput, calls=%fused_computation | convolution fusion | flops 134283264 | bytes 1441792 | tf_op jit(solution)/shard_map/dot_general | solution.py:220
  (1 shorter events, 0.0 us)
Async XLA Ops:
  0.0 69.7 %copy-start = (bf16[1024,512]{1,0:T(8,128)(2,1)S(1)}, bf16[1024,512]{1,0:T(8,128)(2,1)}, u32[]{:S(2)}) copy-start(bf16[1024,512]{1,0:T(8,128)(2,1)} %param.11) | copy-start | bytes 3145732
  2.4 32.2 %all-to-all-start = ((s32[8,1,128]{2,1,0:T(1,128)}), s32[8,1,128]{2,1,0:T(1,128)S(1)}, u32[]{:S(2)}, u32[]{:S(2)}) async-start(s32[8,1,128]{2,1,0:T(1,128)} %get-tuple-element.14), calls=%async_computation | async-start | bytes 8192 | tf_op jit(solution)/shard_map/all_to_all | solution.py:190

commit v3 on v2

--- a/solution.py
+++ b/solution.py
@@ -34,7 +34,8 @@
     value_hbm,
     query_hbm,
     slope_hbm,
-    wanted_ref,
+    listed_ref,
+    rank_ref,
     packed_ref,
     queries_ref,
     near_choice_ref,
@@ -58,17 +59,33 @@
         copy.start()
     copies[0].wait()
     blocks_here, topk = choice_ref.shape
-    shape = wanted_ref.shape
+    members = lax.axis_size(GATHERED)
+    shape = (columns, rank_ref.shape[2])
     column = lax.broadcasted_iota(jnp.int32, shape, 0)
-    member = lax.broadcasted_iota(jnp.int32, shape, 2)
+    member = lax.broadcasted_iota(jnp.int32, shape, 1)
     owner = (member // cores) * (columns * cores) + column * cores + member % cores
+    device = choice_ref[0, 0] // blocks_here
+    far_owner = (member < members) & (column != (device // cores) % columns)
     wanted = jnp.full(shape, -1, jnp.int32)
     for g in range(blocks_here):
         for n in range(1, topk):
             chosen = choice_ref[g, n]
             named = jnp.where(chosen >= 0, chosen // blocks_here, -1)
-            wanted = jnp.where(owner == named, chosen % blocks_here, wanted)
-    wanted_ref[...] = wanted
+            wanted = jnp.where(far_owner & (owner == named), chosen % blocks_here, wanted)
+    needed = wanted >= 0
+    upto = needed.astype(jnp.int32)
+    step = 1
+    while step < members:
+        upto = upto + jnp.where(member >= step, pltpu.roll(upto, step, 1), 0)
+        step *= 2
+    rank = jnp.where(needed, upto - 1, members)
+    row = member * blocks_here + wanted
+    listed = jnp.full(shape, jnp.max(upto), jnp.int32)
+    for place in range(members):
+        found = jnp.sum(jnp.where(rank == place, row, 0), axis=1, keepdims=True)
+        listed = jnp.where(member == place, found, listed)
+    listed_ref[...] = listed.reshape(listed_ref.shape)
+    rank_ref[...] = rank.reshape(rank_ref.shape)
     for copy in copies[1:4]:
         copy.wait()
     packed = lax.dot_general(
@@ -84,19 +101,28 @@
     queries_ref[...] = queries.astype(queries_ref.dtype)
 
 
-def select_kernel(blocks_here, asked_ref, gathered_ref, outgoing_ref):
-    columns, members = outgoing_ref.shape[:2]
+def longest_kernel(limit, listed_ref, over_ref):
+    columns = listed_ref.shape[0]
+    longest = listed_ref[0, 0, 2 * limit]
+    for column in range(1, columns):
+        longest = jnp.maximum(longest, listed_ref[column, 0, 2 * limit])
+    over_ref[0] = (longest > limit).astype(jnp.int32)
+
+
+def select_kernel(listed_ref, gathered_ref, outgoing_ref):
+    columns, places = outgoing_ref.shape[:2]
 
     @pl.loop(0, columns)
     def _(column):
-        for member in range(members):
-            local = jnp.maximum(asked_ref[column, 0, member], 0)
-            outgoing_ref[column, member] = gathered_ref[member * blocks_here + local]
-
-
-def attend_kernel(columns, cores, choice_ref, slope_ref, queries_ref, own_ref, incoming_ref, out_ref):
+        for place in range(places):
+            outgoing_ref[column, place] = gathered_ref[listed_ref[column, 0, place]]
+
+
+def attend_kernel(
+    cores, choice_ref, slope_ref, rank_ref, queries_ref, gathered_ref, incoming_ref, out_ref
+):
     blocks_here, topk = choice_ref.shape
-    members = incoming_ref.shape[0] // columns
+    columns, places = incoming_ref.shape[:2]
     heads = queries_ref.shape[1] // HEAD
     keys = topk * BLOCK
     device = choice_ref[0, 0] // blocks_here
@@ -113,7 +139,10 @@
             local = safe % blocks_here
             column = (owner // cores) % columns
             member = owner // (columns * cores) * cores + owner % cores
-            block = jnp.where(owner == device, own_ref[local], incoming_ref[column * members + member])
+            here = column == (device // cores) % columns
+            place = jnp.minimum(rank_ref[column, 0, member], places - 1)
+            row = jnp.where(here, member * blocks_here + local, 0)
+            block = jnp.where(here, gathered_ref[row], incoming_ref[column, place])
             picked.append(block)
             first = jnp.where(chosen >= 0, chosen * BLOCK, FAR_POSITION)
             key_pos = jnp.where(key_lane // BLOCK == n, first, key_pos)
@@ -159,9 +188,10 @@
     columns = lax.axis_size(SELECTED)
     cores = lax.axis_size("core")
     members = lax.axis_size(GATHERED)
-    wanted, packed, queries, choice, slope = pl.pallas_call(
+    listed, rank, packed, queries, choice, slope = pl.pallas_call(
         functools.partial(prepare_kernel, columns, cores),
         out_shape=(
+            jax.ShapeDtypeStruct((columns, 1, 128), jnp.int32),
             jax.ShapeDtypeStruct((columns, 1, 128), jnp.int32),
             jax.ShapeDtypeStruct((rows, 2 * HEAD), jnp.bfloat16),
             jax.ShapeDtypeStruct((rows, query_weight.shape[1]), jnp.bfloat16),
@@ -169,7 +199,7 @@
             jax.ShapeDtypeStruct(alibi_slope.shape, jnp.float32),
         ),
         in_specs=[HBM] * 6,
-        out_specs=(VMEM,) * 5,
+        out_specs=(VMEM,) * 6,
         scratch_shapes=[
             pltpu.SMEM(block_choice.shape, jnp.int32),
             pltpu.VMEM(tokens.shape, jnp.bfloat16),
@@ -187,30 +217,48 @@
         in_hbm(query_weight),
         in_hbm(alibi_slope),
     )
-    asked = lax.all_to_all(wanted, SELECTED, 0, 0, tiled=True)
+    asked = lax.all_to_all(listed, SELECTED, 0, 0, tiled=True)
     gathered = lax.all_gather(packed, GATHERED, axis=0, tiled=True)
-    outgoing = pl.pallas_call(
-        functools.partial(select_kernel, blocks_here),
-        out_shape=jax.ShapeDtypeStruct((columns, members, BLOCK, 2 * HEAD), jnp.bfloat16),
-        in_specs=[SMEM, VMEM],
-        out_specs=VMEM,
-        name="select",
+    gathered = gathered.reshape(members * blocks_here, BLOCK, 2 * HEAD)
+    limit = members // 2
+    over = pl.pallas_call(
+        functools.partial(longest_kernel, limit),
+        out_shape=jax.ShapeDtypeStruct((1,), jnp.int32),
+        in_specs=[SMEM],
+        out_specs=SMEM,
+        name="longest",
         compiler_params=GRANT,
-    )(asked, gathered.reshape(members * blocks_here, BLOCK, 2 * HEAD))
-    incoming = lax.all_to_all(outgoing, SELECTED, 0, 0, tiled=True)
-    attended = pl.pallas_call(
-        functools.partial(attend_kernel, columns, cores),
-        out_shape=jax.ShapeDtypeStruct(queries.shape, jnp.bfloat16),
-        in_specs=[SMEM, SMEM, VMEM, VMEM, VMEM],
-        out_specs=VMEM,
-        name="attend",
-        compiler_params=GRANT,
-    )(
+    )(asked)
+
+    def attend(places, asked, choice, slope, rank, queries, gathered):
+        outgoing = pl.pallas_call(
+            select_kernel,
+            out_shape=jax.ShapeDtypeStruct((columns, places, BLOCK, 2 * HEAD), jnp.bfloat16),
+            in_specs=[SMEM, VMEM],
+            out_specs=VMEM,
+            name="select",
+            compiler_params=GRANT,
+        )(asked, gathered)
+        incoming = lax.all_to_all(outgoing, SELECTED, 0, 0, tiled=True)
+        return pl.pallas_call(
+            functools.partial(attend_kernel, cores),
+            out_shape=jax.ShapeDtypeStruct(queries.shape, jnp.bfloat16),
+            in_specs=[SMEM, SMEM, SMEM, VMEM, VMEM, VMEM],
+            out_specs=VMEM,
+            name="attend",
+            compiler_params=GRANT,
+        )(choice, slope, rank, queries, gathered, incoming)
+
+    attended = lax.cond(
+        over[0] > 0,
+        functools.partial(attend, members),
+        functools.partial(attend, limit),
+        asked,
         choice,
         slope,
+        rank,
         queries,
-        packed.reshape(blocks_here, BLOCK, 2 * HEAD),
-        incoming.reshape(columns * members, BLOCK, 2 * HEAD),
+        gathered,
     )
     peers = lax.axis_size("tp")
     everyone = lax.all_to_all(

time: 71 us -> 67.4 us (0.949)
  blocking collectives: 58.8 us -> 53.2 us
  Pallas kernels: 5.05 us -> 6.45 us
    all_to_all x1, blocking collectives: 22.3 us -> 16.7 us  [attend(): incoming = lax.all_to_all(outgoing, SELECTED, 0, 0, tiled=True)]
    pallas_call x2 -> x3, Pallas kernels: 2.68 us -> 3.84 us  [the longest x1 2 us: attend(): pl.pallas_call(functools.partial(attend_kernel, cores), out_shape=jax.Sha...]
where the time goes in v3:
time: 67.4 us; the launch traced here: 67.2 us
  blocking collectives  53.2 us (79%)
  Pallas kernels  6.45 us (10%)
  starting transfers between devices  5.67 us (8%)
  matrix products  1.01 us (1%)
  between operations  0.69 us (1%)
    all_gather x1, blocking collectives, shards(): gathered = lax.all_gather(packed, GATHERED, axis=0, tiled=True)  26.5 us
    all_to_all x1, blocking collectives, attend(): incoming = lax.all_to_all(outgoing, SELECTED, 0, 0, tiled=True)  16.7 us
    all_to_all x1, blocking collectives, shards(): lax.all_to_all(jnp.broadcast_to(attended[None], (peers, *attended.shape))...  9.93 us
    all_to_all x1, starting transfers between devices, shards(): asked = lax.all_to_all(listed, SELECTED, 0, 0, tiled=True)  5.67 us
    pallas_call x1, Pallas kernels, shards(): pl.pallas_call(functools.partial(prepare_kernel, columns, cores), out_sha...  2.61 us
    pallas_call x1, Pallas kernels, attend(): pl.pallas_call(functools.partial(attend_kernel, cores), out_shape=jax.Sha...  2 us
  transfers between devices with their start and end apart: 1, of which 0 were waited for; matrix products, arithmetic and copies ran while one was open for 0% of the time, Pallas kernels for 0%

profile of v3, /device:TPU:8, one launch (start us, length us, event | category | flops | bytes accessed | tf_op | source)
XLA Modules:
  0.0 67.2 jit_solution(17884895667283251595)
XLA Ops:
  0.0 0.0 copy-start
  0.0 2.6 %prepare.1 = (s32[8,1,128]{2,1,0:T(1,128)}, s32[8,1,128]{2,1,0:T(1,128)S(1)}, bf16[128,128]{1,0:T(8,128)(2,1)S(1)}, bf16[128,256]{1,0:T(8,128)(2,1)S(1)}, s32[4,8]{1,0:T(4,128)S(1)}, /*index=5*/f32[4]{0:T(128)S(1)}) custom-call(s32[4,8]{1,0:T(4,128)} %choice_hbm.1, bf16[128,2048]{1,0:T(8,128)(2,1)} %tokens_hbm.1, bf16[64,2048]{1,0:T(8,128)(2,1)} %bitcast.12, ...), custom_call_target="tpu_custom_call" | custom-call | tf_op jit(solution)/shard_map/prepare/pallas_call | solution.py:191
  2.6 5.7 %all-to-all-start.2 = ((s32[8,1,128]{2,1,0:T(1,128)}), s32[8,1,128]{2,1,0:T(1,128)S(1)}, u32[]{:S(2)}, u32[]{:S(2)}) async-start(s32[8,1,128]{2,1,0:T(1,128)} %get-tuple-element.50), calls=%async_computation.2 | async-start | bytes 8192 | tf_op jit(solution)/shard_map/all_to_all | solution.py:220
  8.3 26.5 %all_gather.3 = bf16[2048,128]{1,0:T(8,128)(2,1)S(1)} all-gather(bf16[128,128]{1,0:T(8,128)(2,1)S(1)} %get-tuple-element.51), channel_id=1, replica_groups=mesh['z_far'=8,'z_near'=2,'x'=4,'core'=2,'tp'=4] {'z_far','core'}, dimensions={0}, use_global_device_ids=true | all-gather | bytes 557056 | tf_op jit(solution)/shard_map/all_gather | solution.py:221
  34.8 0.0 all-to-all-done.2.listed_ref
  34.8 1.1 %longest.1 = s32[1]{0:T(128)} custom-call(s32[8,1,128]{2,1,0:T(1,128)S(1)} %all-to-all-done.2.listed_ref), custom_call_target="tpu_custom_call" | custom-call | tf_op jit(solution)/shard_map/longest/pallas_call | solution.py:224
  36.6 19.5 %conditional.1 = (bf16[128,256]{1,0:T(8,128)(2,1)S(1)}) conditional(s32[]{:T(128)} %bitcast.2, (s32[8,1,128]{2,1,0:T(1,128)S(1)}, bf16[64,32,128]{2,1,0:T(8,128)(2,1)S(1)}, s32[4,8]{1,0:T(4,128)S(1)}, f32[4]{0:T(128)S(1)}, s32[8,1,128]{2,1,0:T(1,128)S(1)}, /*index=5*/bf16[128,256]{1,0:T(8,128)(2,1)S(1)}) %tuple.14, (s32[8,1,128]{2,1,0:T(1,128)S(1)}, ...), branch_computations={%region_0.0_spmd, %region_1.0_spmd} | conditional | bytes 2097160 | solution.py:252
  36.6 0.7 %select.2 = bf16[8,8,32,128]{3,2,1,0:T(8,128)(2,1)S(1)} custom-call(s32[8,1,128]{2,1,0:T(1,128)S(1)} %get-tuple-element.37.listed_ref, bf16[64,32,128]{2,1,0:T(8,128)(2,1)S(1)} %get-tuple-element.36.gathered_ref), custom_call_target="tpu_custom_call" | custom-call | tf_op jit(solution)/shard_map/cond/branch_0_fun/select/pallas_call | solution.py:234
  37.4 16.7 %all_to_all.18.incoming_ref = bf16[8,8,32,128]{3,2,1,0:T(8,128)(2,1)S(1)} all-to-all(bf16[8,8,32,128]{3,2,1,0:T(8,128)(2,1)S(1)} %select.2), channel_id=1, replica_groups=mesh['z_far'=8,'z_near'=2,'x'=4,'core'=2,'tp'=4] {'z_near','x'}, dimensions={0} | all-to-all | bytes 1048576 | tf_op jit(solution)/shard_map/cond/branch_0_fun/all_to_all | solution.py:242
  54.1 2.0 %attend.2 = bf16[128,256]{1,0:T(8,128)(2,1)S(1)} custom-call(s32[4,8]{1,0:T(4,128)S(1)} %get-tuple-element.32.choice_ref, f32[4]{0:T(128)S(1)} %get-tuple-element.33.slope_ref, s32[8,1,128]{2,1,0:T(1,128)S(1)} %get-tuple-element.34.rank_ref, bf16[128,256]{1,0:T(8,128)(2,1)S(1)} %get-tuple-element.35.queries_ref, ...), custom_call_target="tpu_custom_call" | custom-call | tf_op jit(solution)/shard_map/cond/branch_0_fun/attend/pallas_call | solution.py:243
  56.1 0.1 copy.8
  56.3 9.9 %all_to_all.20 = bf16[4,128,256]{1,2,0:T(8,128)(2,1)S(1)} all-to-all(bf16[4,128,256]{1,2,0:T(8,128)(2,1)S(1)} %broadcast_in_dim.2), channel_id=1, replica_groups=mesh['z_far'=8,'z_near'=2,'x'=4,'core'=2,'tp'=4] {'tp'}, dimensions={0} | all-to-all | bytes 524288 | tf_op jit(solution)/shard_map/all_to_all | solution.py:264
  66.2 0.0 copy-done
  66.2 1.0 %convolution_convert_fusion = bf16[128,512]{1,0:T(8,128)(2,1)} fusion(bf16[128,1024]{0,1:T(8,128)(2,1)S(1)} %bitcast.11, bf16[1024,512]{1,0:T(8,128)(2,1)S(1)} %copy-done), kind=kOutput, calls=%fused_computation | convolution fusion | flops 134283264 | bytes 1441792 | tf_op jit(solution)/shard_map/dot_general | solution.py:268
  (1 shorter events, 0.0 us)
Async XLA Ops:
  0.0 66.2 %copy-start = (bf16[1024,512]{1,0:T(8,128)(2,1)S(1)}, bf16[1024,512]{1,0:T(8,128)(2,1)}, u32[]{:S(2)}) copy-start(bf16[1024,512]{1,0:T(8,128)(2,1)} %param.13) | copy-start | bytes 3145732
  2.6 32.2 %all-to-all-start.2 = ((s32[8,1,128]{2,1,0:T(1,128)}), s32[8,1,128]{2,1,0:T(1,128)S(1)}, u32[]{:S(2)}, u32[]{:S(2)}) async-start(s32[8,1,128]{2,1,0:T(1,128)} %get-tuple-element.50), calls=%async_computation.2 | async-start | bytes 8192 | tf_op jit(solution)/shard_map/all_to_all | solution.py:220

commit v4 on v3

--- a/solution.py
+++ b/solution.py
@@ -38,9 +38,9 @@
     rank_ref,
     packed_ref,
     queries_ref,
-    near_choice_ref,
-    near_slope_ref,
     choice_ref,
+    slope_ref,
+    place_ref,
     tokens_ref,
     packed_weight_ref,
     query_weight_ref,
@@ -52,8 +52,7 @@
         pltpu.make_async_copy(key_hbm, packed_weight_ref.at[pl.ds(0, HEAD)], sems.at[2]),
         pltpu.make_async_copy(value_hbm, packed_weight_ref.at[pl.ds(HEAD, HEAD)], sems.at[3]),
         pltpu.make_async_copy(query_hbm, query_weight_ref, sems.at[4]),
-        pltpu.make_async_copy(choice_hbm, near_choice_ref, sems.at[5]),
-        pltpu.make_async_copy(slope_hbm, near_slope_ref, sems.at[6]),
+        pltpu.make_async_copy(slope_hbm, slope_ref, sems.at[5]),
     ]
     for copy in copies:
         copy.start()
@@ -85,7 +84,9 @@
         found = jnp.sum(jnp.where(rank == place, row, 0), axis=1, keepdims=True)
         listed = jnp.where(member == place, found, listed)
     listed_ref[...] = listed.reshape(listed_ref.shape)
-    rank_ref[...] = rank.reshape(rank_ref.shape)
+    place_ref[...] = rank.reshape(rank_ref.shape)
+    copies.append(pltpu.make_async_copy(place_ref, rank_ref, sems.at[6]))
+    copies[-1].start()
     for copy in copies[1:4]:
         copy.wait()
     packed = lax.dot_general(
@@ -101,16 +102,12 @@
     queries_ref[...] = queries.astype(queries_ref.dtype)
 
 
-def longest_kernel(limit, listed_ref, over_ref):
-    columns = listed_ref.shape[0]
-    longest = listed_ref[0, 0, 2 * limit]
+def select_kernel(listed_ref, gathered_ref, outgoing_ref, over_ref):
+    columns, places = outgoing_ref.shape[:2]
+    longest = listed_ref[0, 0, listed_ref.shape[2] - 1]
     for column in range(1, columns):
-        longest = jnp.maximum(longest, listed_ref[column, 0, 2 * limit])
-    over_ref[0] = (longest > limit).astype(jnp.int32)
-
-
-def select_kernel(listed_ref, gathered_ref, outgoing_ref):
-    columns, places = outgoing_ref.shape[:2]
+        longest = jnp.maximum(longest, listed_ref[column, 0, listed_ref.shape[2] - 1])
+    over_ref[0] = (longest > places).astype(jnp.int32)
 
     @pl.loop(0, columns)
     def _(column):
@@ -192,16 +189,16 @@
         functools.partial(prepare_kernel, columns, cores),
         out_shape=(
             jax.ShapeDtypeStruct((columns, 1, 128), jnp.int32),
-            jax.ShapeDtypeStruct((columns, 1, 128), jnp.int32),
+            pltpu.SMEM((columns, 1, 128), jnp.int32),
             jax.ShapeDtypeStruct((rows, 2 * HEAD), jnp.bfloat16),
             jax.ShapeDtypeStruct((rows, query_weight.shape[1]), jnp.bfloat16),
-            jax.ShapeDtypeStruct(block_choice.shape, jnp.int32),
-            jax.ShapeDtypeStruct(alibi_slope.shape, jnp.float32),
+            pltpu.SMEM(block_choice.shape, jnp.int32),
+            pltpu.SMEM(alibi_slope.shape, jnp.float32),
         ),
         in_specs=[HBM] * 6,
-        out_specs=(VMEM,) * 6,
+        out_specs=(VMEM, SMEM, VMEM, VMEM, SMEM, SMEM),
         scratch_shapes=[
-            pltpu.SMEM(block_choice.shape, jnp.int32),
+            pltpu.VMEM((columns, 1, 128), jnp.int32),
             pltpu.VMEM(tokens.shape, jnp.bfloat16),
             pltpu.VMEM((2 * HEAD, tokens.shape[1]), jnp.bfloat16),
             pltpu.VMEM(query_weight.shape, jnp.bfloat16),
@@ -220,25 +217,20 @@
     asked = lax.all_to_all(listed, SELECTED, 0, 0, tiled=True)
     gathered = lax.all_gather(packed, GATHERED, axis=0, tiled=True)
     gathered = gathered.reshape(members * blocks_here, BLOCK, 2 * HEAD)
-    limit = members // 2
-    over = pl.pallas_call(
-        functools.partial(longest_kernel, limit),
-        out_shape=jax.ShapeDtypeStruct((1,), jnp.int32),
-        in_specs=[SMEM],
-        out_specs=SMEM,
-        name="longest",
-        compiler_params=GRANT,
-    )(asked)
-
-    def attend(places, asked, choice, slope, rank, queries, gathered):
-        outgoing = pl.pallas_call(
+    def select(places, asked, gathered):
+        return pl.pallas_call(
             select_kernel,
-            out_shape=jax.ShapeDtypeStruct((columns, places, BLOCK, 2 * HEAD), jnp.bfloat16),
+            out_shape=(
+                jax.ShapeDtypeStruct((columns, places, BLOCK, 2 * HEAD), jnp.bfloat16),
+                pltpu.SMEM((1,), jnp.int32),
+            ),
             in_specs=[SMEM, VMEM],
-            out_specs=VMEM,
+            out_specs=(VMEM, SMEM),
             name="select",
             compiler_params=GRANT,
         )(asked, gathered)
+
+    def attend(outgoing, choice, slope, rank, queries, gathered):
         incoming = lax.all_to_all(outgoing, SELECTED, 0, 0, tiled=True)
         return pl.pallas_call(
             functools.partial(attend_kernel, cores),
@@ -249,11 +241,19 @@
             compiler_params=GRANT,
         )(choice, slope, rank, queries, gathered, incoming)
 
-    attended = lax.cond(
-        over[0] > 0,
-        functools.partial(attend, members),
-        functools.partial(attend, limit),
+    def short_lists(asked, outgoing, *others):
+        return attend(outgoing, *others)
+
+    def long_lists(asked, outgoing, *others):
+        outgoing, _ = select(members, asked, others[-1])
+        return attend(outgoing, *others)
+
+    outgoing, over = select(members // 2, asked, gathered)
+    attended = lax.switch(
+        over[0],
+        (short_lists, long_lists),
         asked,
+        outgoing,
         choice,
         slope,
         rank,

time: 67.4 us -> 65 us (0.964)
  Pallas kernels: 6.45 us -> 4.68 us
    pallas_call x2 -> x1, Pallas kernels: 1.84 us -> 0.72 us  [select(): pl.pallas_call(select_kernel, out_shape=(jax.ShapeDtypeStruct((columns, p...]
where the time goes in v4:
time: 65 us; the launch traced here: 64.8 us
  blocking collectives  53.2 us (82%)
  starting transfers between devices  5.67 us (9%)
  Pallas kernels  4.68 us (7%)
  matrix products  1.01 us (2%)
    all_gather x1, blocking collectives, shards(): gathered = lax.all_gather(packed, GATHERED, axis=0, tiled=True)  26.5 us
    all_to_all x1, blocking collectives, attend(): incoming = lax.all_to_all(outgoing, SELECTED, 0, 0, tiled=True)  16.7 us
    all_to_all x1, blocking collectives, shards(): lax.all_to_all(jnp.broadcast_to(attended[None], (peers, *attended.shape))...  9.93 us
    all_to_all x1, starting transfers between devices, shards(): asked = lax.all_to_all(listed, SELECTED, 0, 0, tiled=True)  5.67 us
    pallas_call x1, Pallas kernels, shards(): pl.pallas_call(functools.partial(prepare_kernel, columns, cores), out_sha...  2.59 us
    pallas_call x1, Pallas kernels, attend(): pl.pallas_call(functools.partial(attend_kernel, cores), out_shape=jax.Sha...  1.36 us
  transfers between devices with their start and end apart: 1, of which 0 were waited for; matrix products, arithmetic and copies ran while one was open for 0% of the time, Pallas kernels for 0%

profile of v4, /device:TPU:8, one launch (start us, length us, event | category | flops | bytes accessed | tf_op | source)
XLA Modules:
  0.0 64.8 jit_solution(8882443874398578915)
XLA Ops:
  0.0 0.0 copy-start
  0.0 2.6 %prepare.1 = (s32[8,1,128]{2,1,0:T(1,128)}, s32[8,1,128]{2,1,0:T(1,128)S(4)}, bf16[128,128]{1,0:T(8,128)(2,1)S(1)}, bf16[128,256]{1,0:T(8,128)(2,1)S(1)}, s32[4,8]{1,0:T(4,128)S(4)}, /*index=5*/f32[4]{0:T(128)S(4)}) custom-call(s32[4,8]{1,0:T(4,128)} %choice_hbm.1, bf16[128,2048]{1,0:T(8,128)(2,1)} %tokens_hbm.1, bf16[64,2048]{1,0:T(8,128)(2,1)} %bitcast.13, ...), custom_call_target="tpu_custom_call" | custom-call | tf_op jit(solution)/shard_map/prepare/pallas_call | solution.py:188
  2.6 5.7 %all-to-all-start.2 = ((s32[8,1,128]{2,1,0:T(1,128)}), s32[8,1,128]{2,1,0:T(1,128)S(1)}, u32[]{:S(2)}, u32[]{:S(2)}) async-start(s32[8,1,128]{2,1,0:T(1,128)} %get-tuple-element.53), calls=%async_computation.2 | async-start | bytes 8192 | tf_op jit(solution)/shard_map/all_to_all | solution.py:217
  8.3 26.5 %all_gather.3 = bf16[2048,128]{1,0:T(8,128)(2,1)S(1)} all-gather(bf16[128,128]{1,0:T(8,128)(2,1)S(1)} %get-tuple-element.54), channel_id=1, replica_groups=mesh['z_far'=8,'z_near'=2,'x'=4,'core'=2,'tp'=4] {'z_far','core'}, dimensions={0}, use_global_device_ids=true | all-gather | bytes 557056 | tf_op jit(solution)/shard_map/all_gather | solution.py:218
  34.8 0.0 all-to-all-done.2.listed_ref
  34.8 0.7 %select.3 = (bf16[8,8,32,128]{3,2,1,0:T(8,128)(2,1)S(1)}, s32[1]{0:T(128)S(4)}) custom-call(s32[8,1,128]{2,1,0:T(1,128)S(1)} %all-to-all-done.2.listed_ref, bf16[64,32,128]{2,1,0:T(8,128)(2,1)S(1)} %bitcast.9), custom_call_target="tpu_custom_call" | custom-call | tf_op jit(solution)/shard_map/select/pallas_call | solution.py:221
  35.6 18.1 %conditional.1 = (bf16[128,256]{1,0:T(8,128)(2,1)S(1)}) conditional(s32[]{:T(128)} %bitcast.3, (bf16[8,8,32,128]{3,2,1,0:T(8,128)(2,1)S(1)}, s32[4,8]{1,0:T(4,128)S(4)}, f32[4]{0:T(128)S(4)}, s32[8,1,128]{2,1,0:T(1,128)S(4)}, bf16[128,256]{1,0:T(8,128)(2,1)S(1)}, /*index=5*/bf16[64,32,128]{2,1,0:T(8,128)(2,1)S(1)}) %tuple.15, ...), branch_computations={%region_0.0_spmd, %region_1.0_spmd} | conditional | bytes 2097160 | solution.py:252
  35.6 16.7 %all_to_all.18.incoming_ref = bf16[8,8,32,128]{3,2,1,0:T(8,128)(2,1)S(1)} all-to-all(bf16[8,8,32,128]{3,2,1,0:T(8,128)(2,1)S(1)} %get-tuple-element.37), channel_id=1, replica_groups=mesh['z_far'=8,'z_near'=2,'x'=4,'core'=2,'tp'=4] {'z_near','x'}, dimensions={0} | all-to-all | bytes 1048576 | tf_op jit(solution)/shard_map/cond/branch_0_fun/all_to_all | solution.py:234
  52.3 1.4 %attend.2 = bf16[128,256]{1,0:T(8,128)(2,1)S(1)} custom-call(s32[4,8]{1,0:T(4,128)S(4)} %get-tuple-element.32.choice_ref, f32[4]{0:T(128)S(4)} %get-tuple-element.33.slope_ref, s32[8,1,128]{2,1,0:T(1,128)S(4)} %get-tuple-element.34.rank_ref, bf16[128,256]{1,0:T(8,128)(2,1)S(1)} %get-tuple-element.35.queries_ref, ...), custom_call_target="tpu_custom_call" | custom-call | tf_op jit(solution)/shard_map/cond/branch_0_fun/attend/pallas_call | solution.py:235
  53.7 0.1 copy.8
  53.8 9.9 %all_to_all.20 = bf16[4,128,256]{1,2,0:T(8,128)(2,1)S(1)} all-to-all(bf16[4,128,256]{1,2,0:T(8,128)(2,1)S(1)} %broadcast_in_dim.2), channel_id=1, replica_groups=mesh['z_far'=8,'z_near'=2,'x'=4,'core'=2,'tp'=4] {'tp'}, dimensions={0} | all-to-all | bytes 524288 | tf_op jit(solution)/shard_map/all_to_all | solution.py:264
  63.8 0.0 copy-done
  63.8 1.0 %convolution_convert_fusion = bf16[128,512]{1,0:T(8,128)(2,1)} fusion(bf16[128,1024]{0,1:T(8,128)(2,1)S(1)} %bitcast.12, bf16[1024,512]{1,0:T(8,128)(2,1)S(1)} %copy-done), kind=kOutput, calls=%fused_computation | convolution fusion | flops 134283264 | bytes 1441792 | tf_op jit(solution)/shard_map/dot_general | solution.py:268
  (1 shorter events, 0.0 us)
Async XLA Ops:
  0.0 63.8 %copy-start = (bf16[1024,512]{1,0:T(8,128)(2,1)S(1)}, bf16[1024,512]{1,0:T(8,128)(2,1)}, u32[]{:S(2)}) copy-start(bf16[1024,512]{1,0:T(8,128)(2,1)} %param.13) | copy-start | bytes 3145732
  2.6 32.2 %all-to-all-start.2 = ((s32[8,1,128]{2,1,0:T(1,128)}), s32[8,1,128]{2,1,0:T(1,128)S(1)}, u32[]{:S(2)}, u32[]{:S(2)}) async-start(s32[8,1,128]{2,1,0:T(1,128)} %get-tuple-element.53), calls=%async_computation.2 | async-start | bytes 8192 | tf_op jit(solution)/shard_map/all_to_all | solution.py:217

commit v5 on v4

--- a/solution.py
+++ b/solution.py
@@ -34,12 +34,13 @@
     value_hbm,
     query_hbm,
     slope_hbm,
-    listed_ref,
+    listed_hbm,
     rank_ref,
     packed_ref,
     queries_ref,
     choice_ref,
     slope_ref,
+    listed_ref,
     place_ref,
     tokens_ref,
     packed_weight_ref,
@@ -86,7 +87,9 @@
     listed_ref[...] = listed.reshape(listed_ref.shape)
     place_ref[...] = rank.reshape(rank_ref.shape)
     copies.append(pltpu.make_async_copy(place_ref, rank_ref, sems.at[6]))
-    copies[-1].start()
+    copies.append(pltpu.make_async_copy(listed_ref, listed_hbm, sems.at[7]))
+    for copy in copies[-2:]:
+        copy.start()
     for copy in copies[1:4]:
         copy.wait()
     packed = lax.dot_general(
@@ -96,10 +99,11 @@
         preferred_element_type=jnp.float32,
     )
     packed_ref[...] = packed.astype(packed_ref.dtype)
-    for copy in copies[4:]:
-        copy.wait()
+    copies[4].wait()
     queries = jnp.dot(tokens_ref[...], query_weight_ref[...], preferred_element_type=jnp.float32)
     queries_ref[...] = queries.astype(queries_ref.dtype)
+    for copy in copies[5:]:
+        copy.wait()
 
 
 def select_kernel(listed_ref, gathered_ref, outgoing_ref, over_ref):
@@ -174,9 +178,24 @@
         for h in range(0, heads, 2):
             even = pltpu.roll(summed[h * BLOCK : (h + 1) * BLOCK], HEAD, 1)
             odd = summed[(h + 1) * BLOCK : (h + 2) * BLOCK]
-            out_ref[rows, pl.ds(h * HEAD, 2 * HEAD)] = jnp.where(lane < HEAD, even, odd).astype(
-                out_ref.dtype
-            )
+            both = jnp.where(lane < HEAD, even, odd).astype(out_ref.dtype)
+            for peer in range(out_ref.shape[0]):
+                out_ref[peer, rows, pl.ds(h * HEAD, 2 * HEAD)] = both
+
+
+def mix_kernel(attended_ref, weight_ref, mixed_hbm, mixed_ref, sems):
+    peers, _, channels = attended_ref.shape
+    width = mixed_ref.shape[2]
+    attended = jnp.concatenate([attended_ref[p] for p in range(peers)], axis=1)
+    copies = []
+    for half in range(2):
+        cols = pl.ds(half * width, width)
+        mixed = jnp.dot(attended, weight_ref[:, cols], preferred_element_type=jnp.float32)
+        mixed_ref[half] = mixed.astype(mixed_ref.dtype)
+        copies.append(pltpu.make_async_copy(mixed_ref.at[half], mixed_hbm.at[:, cols], sems.at[half]))
+        copies[half].start()
+    for copy in copies:
+        copy.wait()
 
 
 def shards(tokens, query_weight, key_weight, value_weight, out_weight, alibi_slope, block_choice):
@@ -185,6 +204,7 @@
     columns = lax.axis_size(SELECTED)
     cores = lax.axis_size("core")
     members = lax.axis_size(GATHERED)
+    peers = lax.axis_size("tp")
     listed, rank, packed, queries, choice, slope = pl.pallas_call(
         functools.partial(prepare_kernel, columns, cores),
         out_shape=(
@@ -196,13 +216,14 @@
             pltpu.SMEM(alibi_slope.shape, jnp.float32),
         ),
         in_specs=[HBM] * 6,
-        out_specs=(VMEM, SMEM, VMEM, VMEM, SMEM, SMEM),
+        out_specs=(HBM, SMEM, VMEM, VMEM, SMEM, SMEM),
         scratch_shapes=[
+            pltpu.VMEM((columns, 1, 128), jnp.int32),
             pltpu.VMEM((columns, 1, 128), jnp.int32),
             pltpu.VMEM(tokens.shape, jnp.bfloat16),
             pltpu.VMEM((2 * HEAD, tokens.shape[1]), jnp.bfloat16),
             pltpu.VMEM(query_weight.shape, jnp.bfloat16),
-            pltpu.SemaphoreType.DMA((7,)),
+            pltpu.SemaphoreType.DMA((8,)),
         ],
         name="prepare",
         compiler_params=GRANT,
@@ -234,7 +255,7 @@
         incoming = lax.all_to_all(outgoing, SELECTED, 0, 0, tiled=True)
         return pl.pallas_call(
             functools.partial(attend_kernel, cores),
-            out_shape=jax.ShapeDtypeStruct(queries.shape, jnp.bfloat16),
+            out_shape=jax.ShapeDtypeStruct((peers, *queries.shape), jnp.bfloat16),
             in_specs=[SMEM, SMEM, SMEM, VMEM, VMEM, VMEM],
             out_specs=VMEM,
             name="attend",
@@ -260,13 +281,20 @@
         queries,
         gathered,
     )
-    peers = lax.axis_size("tp")
-    everyone = lax.all_to_all(
-        jnp.broadcast_to(attended[None], (peers, *attended.shape)), "tp", 0, 0, tiled=True
-    )
-    everyone = jnp.moveaxis(everyone, 0, 1).reshape(rows, -1)
-    result = jnp.dot(everyone, out_weight, preferred_element_type=jnp.float32)
-    return result.astype(jnp.bfloat16)
+    everyone = lax.all_to_all(attended, "tp", 0, 0, tiled=True)
+    width = out_weight.shape[1]
+    return pl.pallas_call(
+        mix_kernel,
+        out_shape=jax.ShapeDtypeStruct((rows, width), jnp.bfloat16),
+        in_specs=[VMEM, VMEM],
+        out_specs=HBM,
+        scratch_shapes=[
+            pltpu.VMEM((2, rows, width // 2), jnp.bfloat16),
+            pltpu.SemaphoreType.DMA((2,)),
+        ],
+        name="mix",
+        compiler_params=GRANT,
+    )(everyone, out_weight)
 
 
 def solution(mesh):

time: 65 us -> 64.7 us (level)
  matrix products: 1.01 us -> 0 us
  Pallas kernels: 4.68 us -> 5.35 us
    dot_general x1 -> x0, matrix products: 1.01 us -> none  [shards(): result = jnp.dot(everyone, out_weight, preferred_element_type=jnp.float32)]
    pallas_call x0 -> x1, Pallas kernels: none -> 0.97 us  [shards(): pl.pallas_call(mix_kernel, out_shape=jax.ShapeDtypeStruct((rows, width),...]
where the time goes in v5:
time: 64.7 us; the launch traced here: 64.4 us
  blocking collectives  53.3 us (82%)
  starting transfers between devices  5.67 us (9%)
  Pallas kernels  5.35 us (8%)
    all_gather x1, blocking collectives, shards(): gathered = lax.all_gather(packed, GATHERED, axis=0, tiled=True)  26.5 us
    all_to_all x1, blocking collectives, attend(): incoming = lax.all_to_all(outgoing, SELECTED, 0, 0, tiled=True)  16.9 us
    all_to_all x1, blocking collectives, shards(): everyone = lax.all_to_all(attended, 'tp', 0, 0, tiled=True)  9.93 us
    all_to_all x1, starting transfers between devices, shards(): asked = lax.all_to_all(listed, SELECTED, 0, 0, tiled=True)  5.67 us
    pallas_call x1, Pallas kernels, shards(): pl.pallas_call(functools.partial(prepare_kernel, columns, cores), out_sha...  2.29 us
    pallas_call x1, Pallas kernels, attend(): pl.pallas_call(functools.partial(attend_kernel, cores), out_shape=jax.Sha...  1.36 us
  transfers between devices with their start and end apart: 1, of which 0 were waited for; matrix products, arithmetic and copies ran while one was open for 0% of the time, Pallas kernels for 0%

profile of v5, /device:TPU:8, one launch (start us, length us, event | category | flops | bytes accessed | tf_op | source)
XLA Modules:
  0.0 64.4 jit_solution(2982359467651072910)
XLA Ops:
  0.0 2.3 %prepare.1 = (s32[8,1,128]{2,1,0:T(1,128)}, s32[8,1,128]{2,1,0:T(1,128)S(4)}, bf16[128,128]{1,0:T(8,128)(2,1)S(1)}, bf16[128,256]{1,0:T(8,128)(2,1)S(1)}, s32[4,8]{1,0:T(4,128)S(4)}, /*index=5*/f32[4]{0:T(128)S(4)}) custom-call(s32[4,8]{1,0:T(4,128)} %choice_hbm.1, bf16[128,2048]{1,0:T(8,128)(2,1)} %tokens_hbm.1, bf16[64,2048]{1,0:T(8,128)(2,1)} %bitcast.7, ...), custom_call_target="tpu_custom_call" | custom-call | tf_op jit(solution)/shard_map/prepare/pallas_call | solution.py:208
  2.3 5.7 %all-to-all-start.2 = ((s32[8,1,128]{2,1,0:T(1,128)}), s32[8,1,128]{2,1,0:T(1,128)S(1)}, u32[]{:S(2)}, u32[]{:S(2)}) async-start(s32[8,1,128]{2,1,0:T(1,128)} %get-tuple-element.53), calls=%async_computation.2 | async-start | bytes 8192 | tf_op jit(solution)/shard_map/all_to_all | solution.py:238
  8.0 26.5 %all_gather.3 = bf16[2048,128]{1,0:T(8,128)(2,1)S(1)} all-gather(bf16[128,128]{1,0:T(8,128)(2,1)S(1)} %get-tuple-element.54), channel_id=1, replica_groups=mesh['z_far'=8,'z_near'=2,'x'=4,'core'=2,'tp'=4] {'z_far','core'}, dimensions={0}, use_global_device_ids=true | all-gather | bytes 557056 | tf_op jit(solution)/shard_map/all_gather | solution.py:239
  34.5 0.0 all-to-all-done.2.listed_ref
  34.5 0.7 %select.3 = (bf16[8,8,32,128]{3,2,1,0:T(8,128)(2,1)S(1)}, s32[1]{0:T(128)S(4)}) custom-call(s32[8,1,128]{2,1,0:T(1,128)S(1)} %all-to-all-done.2.listed_ref, bf16[64,32,128]{2,1,0:T(8,128)(2,1)S(1)} %bitcast.4), custom_call_target="tpu_custom_call" | custom-call | tf_op jit(solution)/shard_map/select/pallas_call | solution.py:242
  35.3 0.0 copy-start
  35.3 18.2 %conditional.1 = (bf16[4,128,256]{2,1,0:T(8,128)(2,1)S(1)}) conditional(s32[]{:T(128)} %bitcast.3, (bf16[8,8,32,128]{3,2,1,0:T(8,128)(2,1)S(1)}, s32[4,8]{1,0:T(4,128)S(4)}, f32[4]{0:T(128)S(4)}, s32[8,1,128]{2,1,0:T(1,128)S(4)}, bf16[128,256]{1,0:T(8,128)(2,1)S(1)}, /*index=5*/bf16[64,32,128]{2,1,0:T(8,128)(2,1)S(1)}) %tuple.15, ...), branch_computations={%region_0.0_spmd, %region_1.0_spmd} | conditional | bytes 2097160 | solution.py:273
  35.3 16.9 %all_to_all.18.incoming_ref = bf16[8,8,32,128]{3,2,1,0:T(8,128)(2,1)S(1)} all-to-all(bf16[8,8,32,128]{3,2,1,0:T(8,128)(2,1)S(1)} %get-tuple-element.37), channel_id=1, replica_groups=mesh['z_far'=8,'z_near'=2,'x'=4,'core'=2,'tp'=4] {'z_near','x'}, dimensions={0} | all-to-all | bytes 1048576 | tf_op jit(solution)/shard_map/cond/branch_0_fun/all_to_all | solution.py:255
  52.1 1.4 %attend.2 = bf16[4,128,256]{2,1,0:T(8,128)(2,1)S(1)} custom-call(s32[4,8]{1,0:T(4,128)S(4)} %get-tuple-element.32.choice_ref, f32[4]{0:T(128)S(4)} %get-tuple-element.33.slope_ref, s32[8,1,128]{2,1,0:T(1,128)S(4)} %get-tuple-element.34.rank_ref, bf16[128,256]{1,0:T(8,128)(2,1)S(1)} %get-tuple-element.35.queries_ref, ...), custom_call_target="tpu_custom_call" | custom-call | tf_op jit(solution)/shard_map/cond/branch_0_fun/attend/pallas_call | solution.py:256
  53.5 9.9 %all_to_all.20.attended_ref = bf16[4,128,256]{2,1,0:T(8,128)(2,1)S(1)} all-to-all(bf16[4,128,256]{2,1,0:T(8,128)(2,1)S(1)} %get-tuple-element.61), channel_id=1, replica_groups=mesh['z_far'=8,'z_near'=2,'x'=4,'core'=2,'tp'=4] {'tp'}, dimensions={0} | all-to-all | bytes 524288 | tf_op jit(solution)/shard_map/all_to_all | solution.py:284
  63.4 0.0 copy-done
  63.4 1.0 %mix.1 = bf16[128,512]{1,0:T(8,128)(2,1)} custom-call(bf16[4,128,256]{2,1,0:T(8,128)(2,1)S(1)} %all_to_all.20.attended_ref, bf16[1024,512]{1,0:T(8,128)(2,1)S(1)} %copy-done), custom_call_target="tpu_custom_call" | custom-call | tf_op jit(solution)/shard_map/mix/pallas_call | solution.py:286
Async XLA Ops:
  2.3 32.2 %all-to-all-start.2 = ((s32[8,1,128]{2,1,0:T(1,128)}), s32[8,1,128]{2,1,0:T(1,128)S(1)}, u32[]{:S(2)}, u32[]{:S(2)}) async-start(s32[8,1,128]{2,1,0:T(1,128)} %get-tuple-element.53), calls=%async_computation.2 | async-start | bytes 8192 | tf_op jit(solution)/shard_map/all_to_all | solution.py:238
  35.3 28.2 %copy-start = (bf16[1024,512]{1,0:T(8,128)(2,1)S(1)}, bf16[1024,512]{1,0:T(8,128)(2,1)}, u32[]{:S(2)}) copy-start(bf16[1024,512]{1,0:T(8,128)(2,1)} %weight_ref.1) | copy-start | bytes 3145732

commit v6 on v5

--- a/solution.py
+++ b/solution.py
@@ -14,11 +14,26 @@
 GATHERED = ("z_far", "core")
 SELECTED = ("z_near", "x")
 FAR_POSITION = 1 << 20
+PIECES = 4
 
 VMEM = pl.BlockSpec(memory_space=pltpu.VMEM)
 HBM = pl.BlockSpec(memory_space=pltpu.HBM)
 SMEM = pl.BlockSpec(memory_space=pltpu.SMEM)
 GRANT = pltpu.CompilerParams(vmem_limit_bytes=12 << 20)
+
+
+def split(number, by):
+    return number >> (by.bit_length() - 1), number & (by - 1)
+
+
+def in_pieces(source, target, sems):
+    rows = source.shape[0] // len(sems)
+    return [
+        pltpu.make_async_copy(
+            source.at[pl.ds(k * rows, rows)], target.at[pl.ds(k * rows, rows)], sem
+        )
+        for k, sem in enumerate(sems)
+    ]
 
 
 def in_hbm(value):
@@ -47,31 +62,40 @@
     query_weight_ref,
     sems,
 ):
-    copies = [
-        pltpu.make_async_copy(choice_hbm, choice_ref, sems.at[0]),
-        pltpu.make_async_copy(tokens_hbm, tokens_ref, sems.at[1]),
-        pltpu.make_async_copy(key_hbm, packed_weight_ref.at[pl.ds(0, HEAD)], sems.at[2]),
-        pltpu.make_async_copy(value_hbm, packed_weight_ref.at[pl.ds(HEAD, HEAD)], sems.at[3]),
-        pltpu.make_async_copy(query_hbm, query_weight_ref, sems.at[4]),
-        pltpu.make_async_copy(slope_hbm, slope_ref, sems.at[5]),
-    ]
-    for copy in copies:
+    get_choice, get_slope, put_rank, put_listed = (
+        pltpu.make_async_copy(source, target, sems.at[k])
+        for k, (source, target) in enumerate(
+            (
+                (choice_hbm, choice_ref),
+                (slope_hbm, slope_ref),
+                (place_ref, rank_ref),
+                (listed_ref, listed_hbm),
+            )
+        )
+    )
+    pieces = [[sems.at[4 + k * PIECES + n] for n in range(PIECES)] for k in range(4)]
+    get_packed = in_pieces(tokens_hbm, tokens_ref, pieces[0])
+    get_packed += in_pieces(key_hbm, packed_weight_ref.at[pl.ds(0, HEAD)], pieces[1])
+    get_packed += in_pieces(value_hbm, packed_weight_ref.at[pl.ds(HEAD, HEAD)], pieces[2])
+    get_query = in_pieces(query_hbm, query_weight_ref, pieces[3])
+    for copy in [get_choice] + get_packed + get_query + [get_slope]:
         copy.start()
-    copies[0].wait()
+    get_choice.wait()
     blocks_here, topk = choice_ref.shape
     members = lax.axis_size(GATHERED)
     shape = (columns, rank_ref.shape[2])
     column = lax.broadcasted_iota(jnp.int32, shape, 0)
     member = lax.broadcasted_iota(jnp.int32, shape, 1)
-    owner = (member // cores) * (columns * cores) + column * cores + member % cores
-    device = choice_ref[0, 0] // blocks_here
-    far_owner = (member < members) & (column != (device // cores) % columns)
+    far, core = split(member, cores)
+    owner = far * (columns * cores) + column * cores + core
+    device, _ = split(choice_ref[0, 0], blocks_here)
+    far_owner = (member < members) & (column != split(split(device, cores)[0], columns)[1])
     wanted = jnp.full(shape, -1, jnp.int32)
     for g in range(blocks_here):
         for n in range(1, topk):
-            chosen = choice_ref[g, n]
-            named = jnp.where(chosen >= 0, chosen // blocks_here, -1)
-            wanted = jnp.where(far_owner & (owner == named), chosen % blocks_here, wanted)
+            named, local = split(choice_ref[g, n], blocks_here)
+            wanted = jnp.where(owner == named, local, wanted)
+    wanted = jnp.where(far_owner, wanted, -1)
     needed = wanted >= 0
     upto = needed.astype(jnp.int32)
     step = 1
@@ -86,11 +110,9 @@
         listed = jnp.where(member == place, found, listed)
     listed_ref[...] = listed.reshape(listed_ref.shape)
     place_ref[...] = rank.reshape(rank_ref.shape)
-    copies.append(pltpu.make_async_copy(place_ref, rank_ref, sems.at[6]))
-    copies.append(pltpu.make_async_copy(listed_ref, listed_hbm, sems.at[7]))
-    for copy in copies[-2:]:
-        copy.start()
-    for copy in copies[1:4]:
+    put_rank.start()
+    put_listed.start()
+    for copy in get_packed:
         copy.wait()
     packed = lax.dot_general(
         tokens_ref[...],
@@ -99,10 +121,11 @@
         preferred_element_type=jnp.float32,
     )
     packed_ref[...] = packed.astype(packed_ref.dtype)
-    copies[4].wait()
+    for copy in get_query:
+        copy.wait()
     queries = jnp.dot(tokens_ref[...], query_weight_ref[...], preferred_element_type=jnp.float32)
     queries_ref[...] = queries.astype(queries_ref.dtype)
-    for copy in copies[5:]:
+    for copy in (get_slope, put_rank, put_listed):
         copy.wait()
 
 
@@ -126,7 +149,8 @@
     columns, places = incoming_ref.shape[:2]
     heads = queries_ref.shape[1] // HEAD
     keys = topk * BLOCK
-    device = choice_ref[0, 0] // blocks_here
+    device, _ = split(choice_ref[0, 0], blocks_here)
+    own_column = split(split(device, cores)[0], columns)[1]
     lane = lax.broadcasted_iota(jnp.int32, (BLOCK, 2 * HEAD), 1)
     query_row = lax.broadcasted_iota(jnp.int32, (BLOCK, keys), 0)
     key_lane = lax.broadcasted_iota(jnp.int32, (1, keys), 1)
@@ -136,19 +160,19 @@
         for n in range(topk):
             chosen = choice_ref[g, n]
             safe = jnp.maximum(chosen, 0)
-            owner = safe // blocks_here
-            local = safe % blocks_here
-            column = (owner // cores) % columns
-            member = owner // (columns * cores) * cores + owner % cores
-            here = column == (device // cores) % columns
+            owner, local = split(safe, blocks_here)
+            chip, core = split(owner, cores)
+            far, column = split(chip, columns)
+            member = far * cores + core
+            here = column == own_column
             place = jnp.minimum(rank_ref[column, 0, member], places - 1)
             row = jnp.where(here, member * blocks_here + local, 0)
             block = jnp.where(here, gathered_ref[row], incoming_ref[column, place])
             picked.append(block)
             first = jnp.where(chosen >= 0, chosen * BLOCK, FAR_POSITION)
-            key_pos = jnp.where(key_lane // BLOCK == n, first, key_pos)
+            key_pos = jnp.where(split(key_lane, BLOCK)[0] == n, first, key_pos)
         table = jnp.concatenate(picked, axis=0)
-        key_pos = key_pos + key_lane % BLOCK
+        key_pos = key_pos + split(key_lane, BLOCK)[1]
         query_pos = (device * blocks_here + g) * BLOCK + query_row
         distance = query_pos - key_pos
         keep = distance >= 0
@@ -223,7 +247,7 @@
             pltpu.VMEM(tokens.shape, jnp.bfloat16),
             pltpu.VMEM((2 * HEAD, tokens.shape[1]), jnp.bfloat16),
             pltpu.VMEM(query_weight.shape, jnp.bfloat16),
-            pltpu.SemaphoreType.DMA((8,)),
+            pltpu.SemaphoreType.DMA((4 + 4 * PIECES,)),
         ],
         name="prepare",
         compiler_params=GRANT,
@@ -269,7 +293,7 @@
         outgoing, _ = select(members, asked, others[-1])
         return attend(outgoing, *others)
 
-    outgoing, over = select(members // 2, asked, gathered)
+    outgoing, over = select(block_choice.shape[1] - 1, asked, gathered)
     attended = lax.switch(
         over[0],
         (short_lists, long_lists),

time: 64.7 us -> 63.7 us (0.985)
  no operation moved by 1% of the time
where the time goes in v6:
time: 63.7 us; the launch traced here: 63.5 us
  blocking collectives  52.7 us (83%)
  starting transfers between devices  5.67 us (9%)
  Pallas kernels  5.01 us (8%)
    all_gather x1, blocking collectives, shards(): gathered = lax.all_gather(packed, GATHERED, axis=0, tiled=True)  26.5 us
    all_to_all x1, blocking collectives, attend(): incoming = lax.all_to_all(outgoing, SELECTED, 0, 0, tiled=True)  16.3 us
    all_to_all x1, blocking collectives, shards(): everyone = lax.all_to_all(attended, 'tp', 0, 0, tiled=True)  9.93 us
    all_to_all x1, starting transfers between devices, shards(): asked = lax.all_to_all(listed, SELECTED, 0, 0, tiled=True)  5.67 us
    pallas_call x1, Pallas kernels, shards(): pl.pallas_call(functools.partial(prepare_kernel, columns, cores), out_sha...  2.27 us
  transfers between devices with their start and end apart: 1, of which 0 were waited for; matrix products, arithmetic and copies ran while one was open for 0% of the time, Pallas kernels for 0%

profile of v6, /device:TPU:8, one launch (start us, length us, event | category | flops | bytes accessed | tf_op | source)
XLA Modules:
  0.0 63.5 jit_solution(4442718319545527229)
XLA Ops:
  0.0 2.3 %prepare.1 = (s32[8,1,128]{2,1,0:T(1,128)}, s32[8,1,128]{2,1,0:T(1,128)S(4)}, bf16[128,128]{1,0:T(8,128)(2,1)S(1)}, bf16[128,256]{1,0:T(8,128)(2,1)S(1)}, s32[4,8]{1,0:T(4,128)S(4)}, /*index=5*/f32[4]{0:T(128)S(4)}) custom-call(s32[4,8]{1,0:T(4,128)} %choice_hbm.1, bf16[128,2048]{1,0:T(8,128)(2,1)} %tokens_hbm.1, bf16[64,2048]{1,0:T(8,128)(2,1)} %bitcast.7, ...), custom_call_target="tpu_custom_call" | custom-call | tf_op jit(solution)/shard_map/prepare/pallas_call | solution.py:232
  2.3 5.7 %all-to-all-start.2 = ((s32[8,1,128]{2,1,0:T(1,128)}), s32[8,1,128]{2,1,0:T(1,128)S(1)}, u32[]{:S(2)}, u32[]{:S(2)}) async-start(s32[8,1,128]{2,1,0:T(1,128)} %get-tuple-element.53), calls=%async_computation.2 | async-start | bytes 8192 | tf_op jit(solution)/shard_map/all_to_all | solution.py:262
  7.9 26.5 %all_gather.3 = bf16[2048,128]{1,0:T(8,128)(2,1)S(1)} all-gather(bf16[128,128]{1,0:T(8,128)(2,1)S(1)} %get-tuple-element.54), channel_id=1, replica_groups=mesh['z_far'=8,'z_near'=2,'x'=4,'core'=2,'tp'=4] {'z_far','core'}, dimensions={0}, use_global_device_ids=true | all-gather | bytes 557056 | tf_op jit(solution)/shard_map/all_gather | solution.py:263
  34.5 0.0 all-to-all-done.2.listed_ref
  34.5 0.7 %select.3 = (bf16[8,7,32,128]{3,2,1,0:T(8,128)(2,1)S(1)}, s32[1]{0:T(128)S(4)}) custom-call(s32[8,1,128]{2,1,0:T(1,128)S(1)} %all-to-all-done.2.listed_ref, bf16[64,32,128]{2,1,0:T(8,128)(2,1)S(1)} %bitcast.4), custom_call_target="tpu_custom_call" | custom-call | tf_op jit(solution)/shard_map/select/pallas_call | solution.py:266
  35.2 0.0 copy-start
  35.2 17.3 %conditional.1 = (bf16[4,128,256]{2,1,0:T(8,128)(2,1)S(1)}) conditional(s32[]{:T(128)} %bitcast.3, (bf16[8,7,32,128]{3,2,1,0:T(8,128)(2,1)S(1)}, s32[4,8]{1,0:T(4,128)S(4)}, f32[4]{0:T(128)S(4)}, s32[8,1,128]{2,1,0:T(1,128)S(4)}, bf16[128,256]{1,0:T(8,128)(2,1)S(1)}, /*index=5*/bf16[64,32,128]{2,1,0:T(8,128)(2,1)S(1)}) %tuple.15, ...), branch_computations={%region_0.0_spmd, %region_1.0_spmd} | conditional | bytes 2097160 | solution.py:297
  35.2 16.3 %all_to_all.18.incoming_ref = bf16[8,7,32,128]{3,2,1,0:T(8,128)(2,1)S(1)} all-to-all(bf16[8,7,32,128]{3,2,1,0:T(8,128)(2,1)S(1)} %get-tuple-element.37), channel_id=1, replica_groups=mesh['z_far'=8,'z_near'=2,'x'=4,'core'=2,'tp'=4] {'z_near','x'}, dimensions={0} | all-to-all | bytes 917504 | tf_op jit(solution)/shard_map/cond/branch_0_fun/all_to_all | solution.py:279
  51.5 1.1 %attend.2 = bf16[4,128,256]{2,1,0:T(8,128)(2,1)S(1)} custom-call(s32[4,8]{1,0:T(4,128)S(4)} %get-tuple-element.32.choice_ref, f32[4]{0:T(128)S(4)} %get-tuple-element.33.slope_ref, s32[8,1,128]{2,1,0:T(1,128)S(4)} %get-tuple-element.34.rank_ref, bf16[128,256]{1,0:T(8,128)(2,1)S(1)} %get-tuple-element.35.queries_ref, ...), custom_call_target="tpu_custom_call" | custom-call | tf_op jit(solution)/shard_map/cond/branch_0_fun/attend/pallas_call | solution.py:280
  52.6 9.9 %all_to_all.20.attended_ref = bf16[4,128,256]{2,1,0:T(8,128)(2,1)S(1)} all-to-all(bf16[4,128,256]{2,1,0:T(8,128)(2,1)S(1)} %get-tuple-element.61), channel_id=1, replica_groups=mesh['z_far'=8,'z_near'=2,'x'=4,'core'=2,'tp'=4] {'tp'}, dimensions={0} | all-to-all | bytes 524288 | tf_op jit(solution)/shard_map/all_to_all | solution.py:308
  62.5 0.0 copy-done
  62.5 1.0 %mix.1 = bf16[128,512]{1,0:T(8,128)(2,1)} custom-call(bf16[4,128,256]{2,1,0:T(8,128)(2,1)S(1)} %all_to_all.20.attended_ref, bf16[1024,512]{1,0:T(8,128)(2,1)S(1)} %copy-done), custom_call_target="tpu_custom_call" | custom-call | tf_op jit(solution)/shard_map/mix/pallas_call | solution.py:310
Async XLA Ops:
  2.3 32.2 %all-to-all-start.2 = ((s32[8,1,128]{2,1,0:T(1,128)}), s32[8,1,128]{2,1,0:T(1,128)S(1)}, u32[]{:S(2)}, u32[]{:S(2)}) async-start(s32[8,1,128]{2,1,0:T(1,128)} %get-tuple-element.53), calls=%async_computation.2 | async-start | bytes 8192 | tf_op jit(solution)/shard_map/all_to_all | solution.py:262
  35.2 27.3 %copy-start = (bf16[1024,512]{1,0:T(8,128)(2,1)S(1)}, bf16[1024,512]{1,0:T(8,128)(2,1)}, u32[]{:S(2)}) copy-start(bf16[1024,512]{1,0:T(8,128)(2,1)} %weight_ref.1) | copy-start | bytes 3145732

commit v7 on v6

--- a/solution.py
+++ b/solution.py
@@ -24,16 +24,6 @@
 
 def split(number, by):
     return number >> (by.bit_length() - 1), number & (by - 1)
-
-
-def in_pieces(source, target, sems):
-    rows = source.shape[0] // len(sems)
-    return [
-        pltpu.make_async_copy(
-            source.at[pl.ds(k * rows, rows)], target.at[pl.ds(k * rows, rows)], sem
-        )
-        for k, sem in enumerate(sems)
-    ]
 
 
 def in_hbm(value):
@@ -73,13 +63,27 @@
             )
         )
     )
-    pieces = [[sems.at[4 + k * PIECES + n] for n in range(PIECES)] for k in range(4)]
-    get_packed = in_pieces(tokens_hbm, tokens_ref, pieces[0])
-    get_packed += in_pieces(key_hbm, packed_weight_ref.at[pl.ds(0, HEAD)], pieces[1])
-    get_packed += in_pieces(value_hbm, packed_weight_ref.at[pl.ds(HEAD, HEAD)], pieces[2])
-    get_query = in_pieces(query_hbm, query_weight_ref, pieces[3])
-    for copy in [get_choice] + get_packed + get_query + [get_slope]:
-        copy.start()
+    depth = tokens_ref.shape[1] // PIECES
+    pieces = []
+    for k in range(PIECES):
+        cols = pl.ds(k * depth, depth)
+        parts = (
+            (tokens_hbm.at[:, cols], tokens_ref.at[:, cols]),
+            (key_hbm.at[:, cols], packed_weight_ref.at[pl.ds(0, HEAD), cols]),
+            (value_hbm.at[:, cols], packed_weight_ref.at[pl.ds(HEAD, HEAD), cols]),
+            (query_hbm.at[cols], query_weight_ref.at[cols]),
+        )
+        pieces.append(
+            [
+                pltpu.make_async_copy(source, target, sems.at[4 + 4 * k + n])
+                for n, (source, target) in enumerate(parts)
+            ]
+        )
+    get_choice.start()
+    for piece in pieces:
+        for copy in piece:
+            copy.start()
+    get_slope.start()
     get_choice.wait()
     blocks_here, topk = choice_ref.shape
     members = lax.axis_size(GATHERED)
@@ -112,18 +116,21 @@
     place_ref[...] = rank.reshape(rank_ref.shape)
     put_rank.start()
     put_listed.start()
-    for copy in get_packed:
-        copy.wait()
-    packed = lax.dot_general(
-        tokens_ref[...],
-        packed_weight_ref[...],
-        (((1,), (1,)), ((), ())),
-        preferred_element_type=jnp.float32,
-    )
+    packed = queries = 0.0
+    for k, piece in enumerate(pieces):
+        for copy in piece:
+            copy.wait()
+        cols = pl.ds(k * depth, depth)
+        packed += lax.dot_general(
+            tokens_ref[:, cols],
+            packed_weight_ref[:, cols],
+            (((1,), (1,)), ((), ())),
+            preferred_element_type=jnp.float32,
+        )
+        queries += jnp.dot(
+            tokens_ref[:, cols], query_weight_ref[cols], preferred_element_type=jnp.float32
+        )
     packed_ref[...] = packed.astype(packed_ref.dtype)
-    for copy in get_query:
-        copy.wait()
-    queries = jnp.dot(tokens_ref[...], query_weight_ref[...], preferred_element_type=jnp.float32)
     queries_ref[...] = queries.astype(queries_ref.dtype)
     for copy in (get_slope, put_rank, put_listed):
         copy.wait()

time: 63.7 us -> 63.5 us (level)
  no operation moved by 1% of the time
where the time goes in v7:
time: 63.5 us; the launch traced here: 63.2 us
  blocking collectives  52.7 us (83%)
  starting transfers between devices  5.67 us (9%)
  Pallas kernels  4.74 us (7%)
    all_gather x1, blocking collectives, shards(): gathered = lax.all_gather(packed, GATHERED, axis=0, tiled=True)  26.5 us
    all_to_all x1, blocking collectives, attend(): incoming = lax.all_to_all(outgoing, SELECTED, 0, 0, tiled=True)  16.3 us
    all_to_all x1, blocking collectives, shards(): everyone = lax.all_to_all(attended, 'tp', 0, 0, tiled=True)  9.93 us
    all_to_all x1, starting transfers between devices, shards(): asked = lax.all_to_all(listed, SELECTED, 0, 0, tiled=True)  5.67 us
    pallas_call x1, Pallas kernels, shards(): pl.pallas_call(functools.partial(prepare_kernel, columns, cores), out_sha...  2 us
  transfers between devices with their start and end apart: 1, of which 0 were waited for; matrix products, arithmetic and copies ran while one was open for 0% of the time, Pallas kernels for 0%

profile of v7, /device:TPU:8, one launch (start us, length us, event | category | flops | bytes accessed | tf_op | source)
XLA Modules:
  0.0 63.2 jit_solution(266471291025786817)
XLA Ops:
  0.0 2.0 %prepare.1 = (s32[8,1,128]{2,1,0:T(1,128)}, s32[8,1,128]{2,1,0:T(1,128)S(4)}, bf16[128,128]{1,0:T(8,128)(2,1)S(1)}, bf16[128,256]{1,0:T(8,128)(2,1)S(1)}, s32[4,8]{1,0:T(4,128)S(4)}, /*index=5*/f32[4]{0:T(128)S(4)}) custom-call(s32[4,8]{1,0:T(4,128)} %choice_hbm.1, bf16[128,2048]{1,0:T(8,128)(2,1)} %tokens_hbm.1, bf16[64,2048]{1,0:T(8,128)(2,1)} %bitcast.7, ...), custom_call_target="tpu_custom_call" | custom-call | tf_op jit(solution)/shard_map/prepare/pallas_call | solution.py:239
  2.0 5.7 %all-to-all-start.2 = ((s32[8,1,128]{2,1,0:T(1,128)}), s32[8,1,128]{2,1,0:T(1,128)S(1)}, u32[]{:S(2)}, u32[]{:S(2)}) async-start(s32[8,1,128]{2,1,0:T(1,128)} %get-tuple-element.53), calls=%async_computation.2 | async-start | bytes 8192 | tf_op jit(solution)/shard_map/all_to_all | solution.py:269
  7.7 26.5 %all_gather.3 = bf16[2048,128]{1,0:T(8,128)(2,1)S(1)} all-gather(bf16[128,128]{1,0:T(8,128)(2,1)S(1)} %get-tuple-element.54), channel_id=1, replica_groups=mesh['z_far'=8,'z_near'=2,'x'=4,'core'=2,'tp'=4] {'z_far','core'}, dimensions={0}, use_global_device_ids=true | all-gather | bytes 557056 | tf_op jit(solution)/shard_map/all_gather | solution.py:270
  34.2 0.0 all-to-all-done.2.listed_ref
  34.2 0.7 %select.3 = (bf16[8,7,32,128]{3,2,1,0:T(8,128)(2,1)S(1)}, s32[1]{0:T(128)S(4)}) custom-call(s32[8,1,128]{2,1,0:T(1,128)S(1)} %all-to-all-done.2.listed_ref, bf16[64,32,128]{2,1,0:T(8,128)(2,1)S(1)} %bitcast.4), custom_call_target="tpu_custom_call" | custom-call | tf_op jit(solution)/shard_map/select/pallas_call | solution.py:273
  34.9 0.0 copy-start
  35.0 17.3 %conditional.1 = (bf16[4,128,256]{2,1,0:T(8,128)(2,1)S(1)}) conditional(s32[]{:T(128)} %bitcast.3, (bf16[8,7,32,128]{3,2,1,0:T(8,128)(2,1)S(1)}, s32[4,8]{1,0:T(4,128)S(4)}, f32[4]{0:T(128)S(4)}, s32[8,1,128]{2,1,0:T(1,128)S(4)}, bf16[128,256]{1,0:T(8,128)(2,1)S(1)}, /*index=5*/bf16[64,32,128]{2,1,0:T(8,128)(2,1)S(1)}) %tuple.15, ...), branch_computations={%region_0.0_spmd, %region_1.0_spmd} | conditional | bytes 2097160 | solution.py:304
  35.0 16.3 %all_to_all.18.incoming_ref = bf16[8,7,32,128]{3,2,1,0:T(8,128)(2,1)S(1)} all-to-all(bf16[8,7,32,128]{3,2,1,0:T(8,128)(2,1)S(1)} %get-tuple-element.37), channel_id=1, replica_groups=mesh['z_far'=8,'z_near'=2,'x'=4,'core'=2,'tp'=4] {'z_near','x'}, dimensions={0} | all-to-all | bytes 917504 | tf_op jit(solution)/shard_map/cond/branch_0_fun/all_to_all | solution.py:286
  51.2 1.1 %attend.2 = bf16[4,128,256]{2,1,0:T(8,128)(2,1)S(1)} custom-call(s32[4,8]{1,0:T(4,128)S(4)} %get-tuple-element.32.choice_ref, f32[4]{0:T(128)S(4)} %get-tuple-element.33.slope_ref, s32[8,1,128]{2,1,0:T(1,128)S(4)} %get-tuple-element.34.rank_ref, bf16[128,256]{1,0:T(8,128)(2,1)S(1)} %get-tuple-element.35.queries_ref, ...), custom_call_target="tpu_custom_call" | custom-call | tf_op jit(solution)/shard_map/cond/branch_0_fun/attend/pallas_call | solution.py:287
  52.3 9.9 %all_to_all.20.attended_ref = bf16[4,128,256]{2,1,0:T(8,128)(2,1)S(1)} all-to-all(bf16[4,128,256]{2,1,0:T(8,128)(2,1)S(1)} %get-tuple-element.61), channel_id=1, replica_groups=mesh['z_far'=8,'z_near'=2,'x'=4,'core'=2,'tp'=4] {'tp'}, dimensions={0} | all-to-all | bytes 524288 | tf_op jit(solution)/shard_map/all_to_all | solution.py:315
  62.2 0.0 copy-done
  62.2 1.0 %mix.1 = bf16[128,512]{1,0:T(8,128)(2,1)} custom-call(bf16[4,128,256]{2,1,0:T(8,128)(2,1)S(1)} %all_to_all.20.attended_ref, bf16[1024,512]{1,0:T(8,128)(2,1)S(1)} %copy-done), custom_call_target="tpu_custom_call" | custom-call | tf_op jit(solution)/shard_map/mix/pallas_call | solution.py:317
Async XLA Ops:
  2.0 32.2 %all-to-all-start.2 = ((s32[8,1,128]{2,1,0:T(1,128)}), s32[8,1,128]{2,1,0:T(1,128)S(1)}, u32[]{:S(2)}, u32[]{:S(2)}) async-start(s32[8,1,128]{2,1,0:T(1,128)} %get-tuple-element.53), calls=%async_computation.2 | async-start | bytes 8192 | tf_op jit(solution)/shard_map/all_to_all | solution.py:269
  34.9 27.3 %copy-start = (bf16[1024,512]{1,0:T(8,128)(2,1)S(1)}, bf16[1024,512]{1,0:T(8,128)(2,1)}, u32[]{:S(2)}) copy-start(bf16[1024,512]{1,0:T(8,128)(2,1)} %weight_ref.1) | copy-start | bytes 3145732

commit v8 on v7

--- a/solution.py
+++ b/solution.py
@@ -161,6 +161,7 @@
     lane = lax.broadcasted_iota(jnp.int32, (BLOCK, 2 * HEAD), 1)
     query_row = lax.broadcasted_iota(jnp.int32, (BLOCK, keys), 0)
     key_lane = lax.broadcasted_iota(jnp.int32, (1, keys), 1)
+    tables, raws, fars = [], [], []
     for g in range(blocks_here):
         picked = []
         key_pos = jnp.zeros((1, keys), jnp.int32)
@@ -182,8 +183,7 @@
         key_pos = key_pos + split(key_lane, BLOCK)[1]
         query_pos = (device * blocks_here + g) * BLOCK + query_row
         distance = query_pos - key_pos
-        keep = distance >= 0
-        far = distance.astype(jnp.float32)
+        fars.append(jnp.where(distance >= 0, distance.astype(jnp.float32), jnp.inf))
         rows = pl.ds(g * BLOCK, BLOCK)
         padded = []
         for h in range(heads):
@@ -192,20 +192,26 @@
                 pair = pltpu.roll(pair, HEAD, 1)
             padded.append(jnp.where(lane < HEAD, pair, 0.0).astype(jnp.bfloat16))
         query = jnp.concatenate(padded, axis=0)
-        raw = lax.dot_general(
-            query, table, (((1,), (1,)), ((), ())), preferred_element_type=jnp.float32
-        )
+        raws.append(
+            lax.dot_general(
+                query, table, (((1,), (1,)), ((), ())), preferred_element_type=jnp.float32
+            )
+        )
+        tables.append(table)
+    sums = []
+    for table, raw, far in zip(tables, raws, fars):
         weights = []
         for h in range(heads):
             scores = raw[h * BLOCK : (h + 1) * BLOCK] * (HEAD**-0.5) - slope_ref[h] * far
-            scores = jnp.where(keep, scores, -jnp.inf)
             top = jnp.max(scores, axis=1, keepdims=True)
             expd = jnp.exp(scores - top)
             total = jnp.sum(expd, axis=1, keepdims=True)
             weights.append((expd / total).astype(jnp.bfloat16))
-        summed = jnp.dot(
-            jnp.concatenate(weights, axis=0), table, preferred_element_type=jnp.float32
-        )
+        sums.append(
+            jnp.dot(jnp.concatenate(weights, axis=0), table, preferred_element_type=jnp.float32)
+        )
+    for g, summed in enumerate(sums):
+        rows = pl.ds(g * BLOCK, BLOCK)
         for h in range(0, heads, 2):
             even = pltpu.roll(summed[h * BLOCK : (h + 1) * BLOCK], HEAD, 1)
             odd = summed[(h + 1) * BLOCK : (h + 2) * BLOCK]

time: 63.5 us -> 63.3 us (level)
  no operation moved by 1% of the time
where the time goes in v8:
time: 63.3 us; the launch traced here: 63 us
  blocking collectives  52.7 us (83%)
  starting transfers between devices  5.67 us (9%)
  Pallas kernels  4.53 us (7%)
    all_gather x1, blocking collectives, shards(): gathered = lax.all_gather(packed, GATHERED, axis=0, tiled=True)  26.5 us
    all_to_all x1, blocking collectives, attend(): incoming = lax.all_to_all(outgoing, SELECTED, 0, 0, tiled=True)  16.3 us
    all_to_all x1, blocking collectives, shards(): everyone = lax.all_to_all(attended, 'tp', 0, 0, tiled=True)  9.93 us
    all_to_all x1, starting transfers between devices, shards(): asked = lax.all_to_all(listed, SELECTED, 0, 0, tiled=True)  5.67 us
    pallas_call x1, Pallas kernels, shards(): pl.pallas_call(functools.partial(prepare_kernel, columns, cores), out_sha...  2 us
  transfers between devices with their start and end apart: 1, of which 0 were waited for; matrix products, arithmetic and copies ran while one was open for 0% of the time, Pallas kernels for 0%

profile of v8, /device:TPU:8, one launch (start us, length us, event | category | flops | bytes accessed | tf_op | source)
XLA Modules:
  0.0 63.0 jit_solution(12591953842376776217)
XLA Ops:
  0.0 2.0 %prepare.1 = (s32[8,1,128]{2,1,0:T(1,128)}, s32[8,1,128]{2,1,0:T(1,128)S(4)}, bf16[128,128]{1,0:T(8,128)(2,1)S(1)}, bf16[128,256]{1,0:T(8,128)(2,1)S(1)}, s32[4,8]{1,0:T(4,128)S(4)}, /*index=5*/f32[4]{0:T(128)S(4)}) custom-call(s32[4,8]{1,0:T(4,128)} %choice_hbm.1, bf16[128,2048]{1,0:T(8,128)(2,1)} %tokens_hbm.1, bf16[64,2048]{1,0:T(8,128)(2,1)} %bitcast.7, ...), custom_call_target="tpu_custom_call" | custom-call | tf_op jit(solution)/shard_map/prepare/pallas_call | solution.py:245
  2.0 5.7 %all-to-all-start.2 = ((s32[8,1,128]{2,1,0:T(1,128)}), s32[8,1,128]{2,1,0:T(1,128)S(1)}, u32[]{:S(2)}, u32[]{:S(2)}) async-start(s32[8,1,128]{2,1,0:T(1,128)} %get-tuple-element.53), calls=%async_computation.2 | async-start | bytes 8192 | tf_op jit(solution)/shard_map/all_to_all | solution.py:275
  7.7 26.5 %all_gather.3 = bf16[2048,128]{1,0:T(8,128)(2,1)S(1)} all-gather(bf16[128,128]{1,0:T(8,128)(2,1)S(1)} %get-tuple-element.54), channel_id=1, replica_groups=mesh['z_far'=8,'z_near'=2,'x'=4,'core'=2,'tp'=4] {'z_far','core'}, dimensions={0}, use_global_device_ids=true | all-gather | bytes 557056 | tf_op jit(solution)/shard_map/all_gather | solution.py:276
  34.2 0.0 all-to-all-done.2.listed_ref
  34.2 0.7 %select.3 = (bf16[8,7,32,128]{3,2,1,0:T(8,128)(2,1)S(1)}, s32[1]{0:T(128)S(4)}) custom-call(s32[8,1,128]{2,1,0:T(1,128)S(1)} %all-to-all-done.2.listed_ref, bf16[64,32,128]{2,1,0:T(8,128)(2,1)S(1)} %bitcast.4), custom_call_target="tpu_custom_call" | custom-call | tf_op jit(solution)/shard_map/select/pallas_call | solution.py:279
  34.9 0.0 copy-start
  35.0 17.1 %conditional.1 = (bf16[4,128,256]{2,1,0:T(8,128)(2,1)S(1)}) conditional(s32[]{:T(128)} %bitcast.3, (bf16[8,7,32,128]{3,2,1,0:T(8,128)(2,1)S(1)}, s32[4,8]{1,0:T(4,128)S(4)}, f32[4]{0:T(128)S(4)}, s32[8,1,128]{2,1,0:T(1,128)S(4)}, bf16[128,256]{1,0:T(8,128)(2,1)S(1)}, /*index=5*/bf16[64,32,128]{2,1,0:T(8,128)(2,1)S(1)}) %tuple.15, ...), branch_computations={%region_0.0_spmd, %region_1.0_spmd} | conditional | bytes 2097160 | solution.py:310
  35.0 16.3 %all_to_all.18.incoming_ref = bf16[8,7,32,128]{3,2,1,0:T(8,128)(2,1)S(1)} all-to-all(bf16[8,7,32,128]{3,2,1,0:T(8,128)(2,1)S(1)} %get-tuple-element.37), channel_id=1, replica_groups=mesh['z_far'=8,'z_near'=2,'x'=4,'core'=2,'tp'=4] {'z_near','x'}, dimensions={0} | all-to-all | bytes 917504 | tf_op jit(solution)/shard_map/cond/branch_0_fun/all_to_all | solution.py:292
  51.2 0.8 %attend.2 = bf16[4,128,256]{2,1,0:T(8,128)(2,1)S(1)} custom-call(s32[4,8]{1,0:T(4,128)S(4)} %get-tuple-element.32.choice_ref, f32[4]{0:T(128)S(4)} %get-tuple-element.33.slope_ref, s32[8,1,128]{2,1,0:T(1,128)S(4)} %get-tuple-element.34.rank_ref, bf16[128,256]{1,0:T(8,128)(2,1)S(1)} %get-tuple-element.35.queries_ref, ...), custom_call_target="tpu_custom_call" | custom-call | tf_op jit(solution)/shard_map/cond/branch_0_fun/attend/pallas_call | solution.py:293
  52.1 9.9 %all_to_all.20.attended_ref = bf16[4,128,256]{2,1,0:T(8,128)(2,1)S(1)} all-to-all(bf16[4,128,256]{2,1,0:T(8,128)(2,1)S(1)} %get-tuple-element.61), channel_id=1, replica_groups=mesh['z_far'=8,'z_near'=2,'x'=4,'core'=2,'tp'=4] {'tp'}, dimensions={0} | all-to-all | bytes 524288 | tf_op jit(solution)/shard_map/all_to_all | solution.py:321
  62.0 0.0 copy-done
  62.0 1.0 %mix.1 = bf16[128,512]{1,0:T(8,128)(2,1)} custom-call(bf16[4,128,256]{2,1,0:T(8,128)(2,1)S(1)} %all_to_all.20.attended_ref, bf16[1024,512]{1,0:T(8,128)(2,1)S(1)} %copy-done), custom_call_target="tpu_custom_call" | custom-call | tf_op jit(solution)/shard_map/mix/pallas_call | solution.py:323
Async XLA Ops:
  2.0 32.2 %all-to-all-start.2 = ((s32[8,1,128]{2,1,0:T(1,128)}), s32[8,1,128]{2,1,0:T(1,128)S(1)}, u32[]{:S(2)}, u32[]{:S(2)}) async-start(s32[8,1,128]{2,1,0:T(1,128)} %get-tuple-element.53), calls=%async_computation.2 | async-start | bytes 8192 | tf_op jit(solution)/shard_map/all_to_all | solution.py:275
  34.9 27.1 %copy-start = (bf16[1024,512]{1,0:T(8,128)(2,1)S(1)}, bf16[1024,512]{1,0:T(8,128)(2,1)}, u32[]{:S(2)}) copy-start(bf16[1024,512]{1,0:T(8,128)(2,1)} %weight_ref.1) | copy-start | bytes 3145732

commit v9 on v8

--- a/solution.py
+++ b/solution.py
@@ -143,10 +143,10 @@
         longest = jnp.maximum(longest, listed_ref[column, 0, listed_ref.shape[2] - 1])
     over_ref[0] = (longest > places).astype(jnp.int32)
 
-    @pl.loop(0, columns)
-    def _(column):
-        for place in range(places):
-            outgoing_ref[column, place] = gathered_ref[listed_ref[column, 0, place]]
+    for column in range(columns):
+        blocks = [gathered_ref[listed_ref[column, 0, place]] for place in range(places)]
+        for place, block in enumerate(blocks):
+            outgoing_ref[column, place] = block
 
 
 def attend_kernel(

time: 63.3 us -> 63.2 us (level)
  no operation moved by 1% of the time
where the time goes in v9:
time: 63.2 us; the launch traced here: 62.9 us
  blocking collectives  52.7 us (83%)
  starting transfers between devices  5.67 us (9%)
  Pallas kernels  4.47 us (7%)
    all_gather x1, blocking collectives, shards(): gathered = lax.all_gather(packed, GATHERED, axis=0, tiled=True)  26.5 us
    all_to_all x1, blocking collectives, attend(): incoming = lax.all_to_all(outgoing, SELECTED, 0, 0, tiled=True)  16.3 us
    all_to_all x1, blocking collectives, shards(): everyone = lax.all_to_all(attended, 'tp', 0, 0, tiled=True)  9.93 us
    all_to_all x1, starting transfers between devices, shards(): asked = lax.all_to_all(listed, SELECTED, 0, 0, tiled=True)  5.67 us
    pallas_call x1, Pallas kernels, shards(): pl.pallas_call(functools.partial(prepare_kernel, columns, cores), out_sha...  2 us
  transfers between devices with their start and end apart: 1, of which 0 were waited for; matrix products, arithmetic and copies ran while one was open for 0% of the time, Pallas kernels for 0%

profile of v9, /device:TPU:8, one launch (start us, length us, event | category | flops | bytes accessed | tf_op | source)
XLA Modules:
  0.0 62.9 jit_solution(1064824059357418239)
XLA Ops:
  0.0 2.0 %prepare.1 = (s32[8,1,128]{2,1,0:T(1,128)}, s32[8,1,128]{2,1,0:T(1,128)S(4)}, bf16[128,128]{1,0:T(8,128)(2,1)S(1)}, bf16[128,256]{1,0:T(8,128)(2,1)S(1)}, s32[4,8]{1,0:T(4,128)S(4)}, /*index=5*/f32[4]{0:T(128)S(4)}) custom-call(s32[4,8]{1,0:T(4,128)} %choice_hbm.1, bf16[128,2048]{1,0:T(8,128)(2,1)} %tokens_hbm.1, bf16[64,2048]{1,0:T(8,128)(2,1)} %bitcast.7, ...), custom_call_target="tpu_custom_call" | custom-call | tf_op jit(solution)/shard_map/prepare/pallas_call | solution.py:245
  2.0 5.7 %all-to-all-start.2 = ((s32[8,1,128]{2,1,0:T(1,128)}), s32[8,1,128]{2,1,0:T(1,128)S(1)}, u32[]{:S(2)}, u32[]{:S(2)}) async-start(s32[8,1,128]{2,1,0:T(1,128)} %get-tuple-element.53), calls=%async_computation.2 | async-start | bytes 8192 | tf_op jit(solution)/shard_map/all_to_all | solution.py:275
  7.7 26.5 %all_gather.3 = bf16[2048,128]{1,0:T(8,128)(2,1)S(1)} all-gather(bf16[128,128]{1,0:T(8,128)(2,1)S(1)} %get-tuple-element.54), channel_id=1, replica_groups=mesh['z_far'=8,'z_near'=2,'x'=4,'core'=2,'tp'=4] {'z_far','core'}, dimensions={0}, use_global_device_ids=true | all-gather | bytes 557056 | tf_op jit(solution)/shard_map/all_gather | solution.py:276
  34.2 0.0 all-to-all-done.2.listed_ref
  34.2 0.7 %select.3 = (bf16[8,7,32,128]{3,2,1,0:T(8,128)(2,1)S(1)}, s32[1]{0:T(128)S(4)}) custom-call(s32[8,1,128]{2,1,0:T(1,128)S(1)} %all-to-all-done.2.listed_ref, bf16[64,32,128]{2,1,0:T(8,128)(2,1)S(1)} %bitcast.4), custom_call_target="tpu_custom_call" | custom-call | tf_op jit(solution)/shard_map/select/pallas_call | solution.py:279
  34.9 0.0 copy-start
  34.9 17.1 %conditional.1 = (bf16[4,128,256]{2,1,0:T(8,128)(2,1)S(1)}) conditional(s32[]{:T(128)} %bitcast.3, (bf16[8,7,32,128]{3,2,1,0:T(8,128)(2,1)S(1)}, s32[4,8]{1,0:T(4,128)S(4)}, f32[4]{0:T(128)S(4)}, s32[8,1,128]{2,1,0:T(1,128)S(4)}, bf16[128,256]{1,0:T(8,128)(2,1)S(1)}, /*index=5*/bf16[64,32,128]{2,1,0:T(8,128)(2,1)S(1)}) %tuple.15, ...), branch_computations={%region_0.0_spmd, %region_1.0_spmd} | conditional | bytes 2097160 | solution.py:310
  34.9 16.3 %all_to_all.18.incoming_ref = bf16[8,7,32,128]{3,2,1,0:T(8,128)(2,1)S(1)} all-to-all(bf16[8,7,32,128]{3,2,1,0:T(8,128)(2,1)S(1)} %get-tuple-element.37), channel_id=1, replica_groups=mesh['z_far'=8,'z_near'=2,'x'=4,'core'=2,'tp'=4] {'z_near','x'}, dimensions={0} | all-to-all | bytes 917504 | tf_op jit(solution)/shard_map/cond/branch_0_fun/all_to_all | solution.py:292
  51.2 0.8 %attend.2 = bf16[4,128,256]{2,1,0:T(8,128)(2,1)S(1)} custom-call(s32[4,8]{1,0:T(4,128)S(4)} %get-tuple-element.32.choice_ref, f32[4]{0:T(128)S(4)} %get-tuple-element.33.slope_ref, s32[8,1,128]{2,1,0:T(1,128)S(4)} %get-tuple-element.34.rank_ref, bf16[128,256]{1,0:T(8,128)(2,1)S(1)} %get-tuple-element.35.queries_ref, ...), custom_call_target="tpu_custom_call" | custom-call | tf_op jit(solution)/shard_map/cond/branch_0_fun/attend/pallas_call | solution.py:293
  52.0 9.9 %all_to_all.20.attended_ref = bf16[4,128,256]{2,1,0:T(8,128)(2,1)S(1)} all-to-all(bf16[4,128,256]{2,1,0:T(8,128)(2,1)S(1)} %get-tuple-element.61), channel_id=1, replica_groups=mesh['z_far'=8,'z_near'=2,'x'=4,'core'=2,'tp'=4] {'tp'}, dimensions={0} | all-to-all | bytes 524288 | tf_op jit(solution)/shard_map/all_to_all | solution.py:321
  62.0 0.0 copy-done
  62.0 1.0 %mix.1 = bf16[128,512]{1,0:T(8,128)(2,1)} custom-call(bf16[4,128,256]{2,1,0:T(8,128)(2,1)S(1)} %all_to_all.20.attended_ref, bf16[1024,512]{1,0:T(8,128)(2,1)S(1)} %copy-done), custom_call_target="tpu_custom_call" | custom-call | tf_op jit(solution)/shard_map/mix/pallas_call | solution.py:323
Async XLA Ops:
  2.0 32.2 %all-to-all-start.2 = ((s32[8,1,128]{2,1,0:T(1,128)}), s32[8,1,128]{2,1,0:T(1,128)S(1)}, u32[]{:S(2)}, u32[]{:S(2)}) async-start(s32[8,1,128]{2,1,0:T(1,128)} %get-tuple-element.53), calls=%async_computation.2 | async-start | bytes 8192 | tf_op jit(solution)/shard_map/all_to_all | solution.py:275
  34.9 27.1 %copy-start = (bf16[1024,512]{1,0:T(8,128)(2,1)S(1)}, bf16[1024,512]{1,0:T(8,128)(2,1)}, u32[]{:S(2)}) copy-start(bf16[1024,512]{1,0:T(8,128)(2,1)} %weight_ref.1) | copy-start | bytes 3145732

commit v10 on v9

--- a/solution.py
+++ b/solution.py
@@ -67,10 +67,14 @@
     pieces = []
     for k in range(PIECES):
         cols = pl.ds(k * depth, depth)
-        parts = (
+        parts = ()
+        if k == 0:
+            parts = (
+                (key_hbm, packed_weight_ref.at[pl.ds(0, HEAD)]),
+                (value_hbm, packed_weight_ref.at[pl.ds(HEAD, HEAD)]),
+            )
+        parts += (
             (tokens_hbm.at[:, cols], tokens_ref.at[:, cols]),
-            (key_hbm.at[:, cols], packed_weight_ref.at[pl.ds(0, HEAD), cols]),
-            (value_hbm.at[:, cols], packed_weight_ref.at[pl.ds(HEAD, HEAD), cols]),
             (query_hbm.at[cols], query_weight_ref.at[cols]),
         )
         pieces.append(

time: 63.2 us -> 63.2 us (level)
  no operation moved by 1% of the time
where the time goes in v10:
time: 63.2 us; the launch traced here: 63 us
  blocking collectives  52.7 us (83%)
  starting transfers between devices  5.67 us (9%)
  Pallas kernels  4.48 us (7%)
    all_gather x1, blocking collectives, shards(): gathered = lax.all_gather(packed, GATHERED, axis=0, tiled=True)  26.5 us
    all_to_all x1, blocking collectives, attend(): incoming = lax.all_to_all(outgoing, SELECTED, 0, 0, tiled=True)  16.3 us
    all_to_all x1, blocking collectives, shards(): everyone = lax.all_to_all(attended, 'tp', 0, 0, tiled=True)  9.94 us
    all_to_all x1, starting transfers between devices, shards(): asked = lax.all_to_all(listed, SELECTED, 0, 0, tiled=True)  5.67 us
    pallas_call x1, Pallas kernels, shards(): pl.pallas_call(functools.partial(prepare_kernel, columns, cores), out_sha...  2.01 us
  transfers between devices with their start and end apart: 1, of which 0 were waited for; matrix products, arithmetic and copies ran while one was open for 0% of the time, Pallas kernels for 0%

profile of v10, /device:TPU:8, one launch (start us, length us, event | category | flops | bytes accessed | tf_op | source)
XLA Modules:
  0.0 63.0 jit_solution(3811821017578542694)
XLA Ops:
  0.0 2.0 %prepare.1 = (s32[8,1,128]{2,1,0:T(1,128)}, s32[8,1,128]{2,1,0:T(1,128)S(4)}, bf16[128,128]{1,0:T(8,128)(2,1)S(1)}, bf16[128,256]{1,0:T(8,128)(2,1)S(1)}, s32[4,8]{1,0:T(4,128)S(4)}, /*index=5*/f32[4]{0:T(128)S(4)}) custom-call(s32[4,8]{1,0:T(4,128)} %choice_hbm.1, bf16[128,2048]{1,0:T(8,128)(2,1)} %tokens_hbm.1, bf16[64,2048]{1,0:T(8,128)(2,1)} %bitcast.7, ...), custom_call_target="tpu_custom_call" | custom-call | tf_op jit(solution)/shard_map/prepare/pallas_call | solution.py:249
  2.0 5.7 %all-to-all-start.2 = ((s32[8,1,128]{2,1,0:T(1,128)}), s32[8,1,128]{2,1,0:T(1,128)S(1)}, u32[]{:S(2)}, u32[]{:S(2)}) async-start(s32[8,1,128]{2,1,0:T(1,128)} %get-tuple-element.53), calls=%async_computation.2 | async-start | bytes 8192 | tf_op jit(solution)/shard_map/all_to_all | solution.py:279
  7.7 26.5 %all_gather.3 = bf16[2048,128]{1,0:T(8,128)(2,1)S(1)} all-gather(bf16[128,128]{1,0:T(8,128)(2,1)S(1)} %get-tuple-element.54), channel_id=1, replica_groups=mesh['z_far'=8,'z_near'=2,'x'=4,'core'=2,'tp'=4] {'z_far','core'}, dimensions={0}, use_global_device_ids=true | all-gather | bytes 557056 | tf_op jit(solution)/shard_map/all_gather | solution.py:280
  34.2 0.0 all-to-all-done.2.listed_ref
  34.2 0.7 %select.3 = (bf16[8,7,32,128]{3,2,1,0:T(8,128)(2,1)S(1)}, s32[1]{0:T(128)S(4)}) custom-call(s32[8,1,128]{2,1,0:T(1,128)S(1)} %all-to-all-done.2.listed_ref, bf16[64,32,128]{2,1,0:T(8,128)(2,1)S(1)} %bitcast.4), custom_call_target="tpu_custom_call" | custom-call | tf_op jit(solution)/shard_map/select/pallas_call | solution.py:283
  34.9 0.0 copy-start
  34.9 17.1 %conditional.1 = (bf16[4,128,256]{2,1,0:T(8,128)(2,1)S(1)}) conditional(s32[]{:T(128)} %bitcast.3, (bf16[8,7,32,128]{3,2,1,0:T(8,128)(2,1)S(1)}, s32[4,8]{1,0:T(4,128)S(4)}, f32[4]{0:T(128)S(4)}, s32[8,1,128]{2,1,0:T(1,128)S(4)}, bf16[128,256]{1,0:T(8,128)(2,1)S(1)}, /*index=5*/bf16[64,32,128]{2,1,0:T(8,128)(2,1)S(1)}) %tuple.15, ...), branch_computations={%region_0.0_spmd, %region_1.0_spmd} | conditional | bytes 2097160 | solution.py:314
  34.9 16.3 %all_to_all.18.incoming_ref = bf16[8,7,32,128]{3,2,1,0:T(8,128)(2,1)S(1)} all-to-all(bf16[8,7,32,128]{3,2,1,0:T(8,128)(2,1)S(1)} %get-tuple-element.37), channel_id=1, replica_groups=mesh['z_far'=8,'z_near'=2,'x'=4,'core'=2,'tp'=4] {'z_near','x'}, dimensions={0} | all-to-all | bytes 917504 | tf_op jit(solution)/shard_map/cond/branch_0_fun/all_to_all | solution.py:296
  51.2 0.8 %attend.2 = bf16[4,128,256]{2,1,0:T(8,128)(2,1)S(1)} custom-call(s32[4,8]{1,0:T(4,128)S(4)} %get-tuple-element.32.choice_ref, f32[4]{0:T(128)S(4)} %get-tuple-element.33.slope_ref, s32[8,1,128]{2,1,0:T(1,128)S(4)} %get-tuple-element.34.rank_ref, bf16[128,256]{1,0:T(8,128)(2,1)S(1)} %get-tuple-element.35.queries_ref, ...), custom_call_target="tpu_custom_call" | custom-call | tf_op jit(solution)/shard_map/cond/branch_0_fun/attend/pallas_call | solution.py:297
  52.0 9.9 %all_to_all.20.attended_ref = bf16[4,128,256]{2,1,0:T(8,128)(2,1)S(1)} all-to-all(bf16[4,128,256]{2,1,0:T(8,128)(2,1)S(1)} %get-tuple-element.61), channel_id=1, replica_groups=mesh['z_far'=8,'z_near'=2,'x'=4,'core'=2,'tp'=4] {'tp'}, dimensions={0} | all-to-all | bytes 524288 | tf_op jit(solution)/shard_map/all_to_all | solution.py:325
  62.0 0.0 copy-done
  62.0 1.0 %mix.1 = bf16[128,512]{1,0:T(8,128)(2,1)} custom-call(bf16[4,128,256]{2,1,0:T(8,128)(2,1)S(1)} %all_to_all.20.attended_ref, bf16[1024,512]{1,0:T(8,128)(2,1)S(1)} %copy-done), custom_call_target="tpu_custom_call" | custom-call | tf_op jit(solution)/shard_map/mix/pallas_call | solution.py:327
Async XLA Ops:
  2.0 32.2 %all-to-all-start.2 = ((s32[8,1,128]{2,1,0:T(1,128)}), s32[8,1,128]{2,1,0:T(1,128)S(1)}, u32[]{:S(2)}, u32[]{:S(2)}) async-start(s32[8,1,128]{2,1,0:T(1,128)} %get-tuple-element.53), calls=%async_computation.2 | async-start | bytes 8192 | tf_op jit(solution)/shard_map/all_to_all | solution.py:279
  34.9 27.1 %copy-start = (bf16[1024,512]{1,0:T(8,128)(2,1)S(1)}, bf16[1024,512]{1,0:T(8,128)(2,1)}, u32[]{:S(2)}) copy-start(bf16[1024,512]{1,0:T(8,128)(2,1)} %weight_ref.1) | copy-start | bytes 3145732

commit v11 on v10

--- a/solution.py
+++ b/solution.py
@@ -221,13 +221,15 @@
             odd = summed[(h + 1) * BLOCK : (h + 2) * BLOCK]
             both = jnp.where(lane < HEAD, even, odd).astype(out_ref.dtype)
             for peer in range(out_ref.shape[0]):
-                out_ref[peer, rows, pl.ds(h * HEAD, 2 * HEAD)] = both
+                out_ref[peer, h // 2, rows] = both
 
 
 def mix_kernel(attended_ref, weight_ref, mixed_hbm, mixed_ref, sems):
-    peers, _, channels = attended_ref.shape
+    peers, pairs = attended_ref.shape[:2]
     width = mixed_ref.shape[2]
-    attended = jnp.concatenate([attended_ref[p] for p in range(peers)], axis=1)
+    attended = jnp.concatenate(
+        [attended_ref[p, i] for p in range(peers) for i in range(pairs)], axis=1
+    )
     copies = []
     for half in range(2):
         cols = pl.ds(half * width, width)
@@ -296,7 +298,9 @@
         incoming = lax.all_to_all(outgoing, SELECTED, 0, 0, tiled=True)
         return pl.pallas_call(
             functools.partial(attend_kernel, cores),
-            out_shape=jax.ShapeDtypeStruct((peers, *queries.shape), jnp.bfloat16),
+            out_shape=jax.ShapeDtypeStruct(
+                (peers, queries.shape[1] // (2 * HEAD), rows, 2 * HEAD), jnp.bfloat16
+            ),
             in_specs=[SMEM, SMEM, SMEM, VMEM, VMEM, VMEM],
             out_specs=VMEM,
             name="attend",

time: 63.2 us -> 63.2 us (level)
  no operation moved by 1% of the time
where the time goes in v11:
time: 63.2 us; the launch traced here: 62.9 us
  blocking collectives  52.7 us (83%)
  starting transfers between devices  5.67 us (9%)
  Pallas kernels  4.48 us (7%)
    all_gather x1, blocking collectives, shards(): gathered = lax.all_gather(packed, GATHERED, axis=0, tiled=True)  26.5 us
    all_to_all x1, blocking collectives, attend(): incoming = lax.all_to_all(outgoing, SELECTED, 0, 0, tiled=True)  16.3 us
    all_to_all x1, blocking collectives, shards(): everyone = lax.all_to_all(attended, 'tp', 0, 0, tiled=True)  9.94 us
    all_to_all x1, starting transfers between devices, shards(): asked = lax.all_to_all(listed, SELECTED, 0, 0, tiled=True)  5.67 us
    pallas_call x1, Pallas kernels, shards(): pl.pallas_call(functools.partial(prepare_kernel, columns, cores), out_sha...  2.01 us
  transfers between devices with their start and end apart: 1, of which 0 were waited for; matrix products, arithmetic and copies ran while one was open for 0% of the time, Pallas kernels for 0%

profile of v11, /device:TPU:8, one launch (start us, length us, event | category | flops | bytes accessed | tf_op | source)
XLA Modules:
  0.0 62.9 jit_solution(10207636923329140822)
XLA Ops:
  0.0 2.0 %prepare.1 = (s32[8,1,128]{2,1,0:T(1,128)}, s32[8,1,128]{2,1,0:T(1,128)S(4)}, bf16[128,128]{1,0:T(8,128)(2,1)S(1)}, bf16[128,256]{1,0:T(8,128)(2,1)S(1)}, s32[4,8]{1,0:T(4,128)S(4)}, /*index=5*/f32[4]{0:T(128)S(4)}) custom-call(s32[4,8]{1,0:T(4,128)} %choice_hbm.1, bf16[128,2048]{1,0:T(8,128)(2,1)} %tokens_hbm.1, bf16[64,2048]{1,0:T(8,128)(2,1)} %bitcast.7, ...), custom_call_target="tpu_custom_call" | custom-call | tf_op jit(solution)/shard_map/prepare/pallas_call | solution.py:251
  2.0 5.7 %all-to-all-start.2 = ((s32[8,1,128]{2,1,0:T(1,128)}), s32[8,1,128]{2,1,0:T(1,128)S(1)}, u32[]{:S(2)}, u32[]{:S(2)}) async-start(s32[8,1,128]{2,1,0:T(1,128)} %get-tuple-element.53), calls=%async_computation.2 | async-start | bytes 8192 | tf_op jit(solution)/shard_map/all_to_all | solution.py:281
  7.7 26.5 %all_gather.3 = bf16[2048,128]{1,0:T(8,128)(2,1)S(1)} all-gather(bf16[128,128]{1,0:T(8,128)(2,1)S(1)} %get-tuple-element.54), channel_id=1, replica_groups=mesh['z_far'=8,'z_near'=2,'x'=4,'core'=2,'tp'=4] {'z_far','core'}, dimensions={0}, use_global_device_ids=true | all-gather | bytes 557056 | tf_op jit(solution)/shard_map/all_gather | solution.py:282
  34.2 0.0 all-to-all-done.2.listed_ref
  34.2 0.7 %select.3 = (bf16[8,7,32,128]{3,2,1,0:T(8,128)(2,1)S(1)}, s32[1]{0:T(128)S(4)}) custom-call(s32[8,1,128]{2,1,0:T(1,128)S(1)} %all-to-all-done.2.listed_ref, bf16[64,32,128]{2,1,0:T(8,128)(2,1)S(1)} %bitcast.4), custom_call_target="tpu_custom_call" | custom-call | tf_op jit(solution)/shard_map/select/pallas_call | solution.py:285
  34.9 0.0 copy-start
  34.9 17.1 %conditional.1 = (bf16[4,2,128,128]{3,2,1,0:T(8,128)(2,1)S(1)}) conditional(s32[]{:T(128)} %bitcast.3, (bf16[8,7,32,128]{3,2,1,0:T(8,128)(2,1)S(1)}, s32[4,8]{1,0:T(4,128)S(4)}, f32[4]{0:T(128)S(4)}, s32[8,1,128]{2,1,0:T(1,128)S(4)}, bf16[128,256]{1,0:T(8,128)(2,1)S(1)}, /*index=5*/bf16[64,32,128]{2,1,0:T(8,128)(2,1)S(1)}) %tuple.15, ...), branch_computations={%region_0.0_spmd, %region_1.0_spmd} | conditional | bytes 2097160 | solution.py:318
  34.9 16.3 %all_to_all.18.incoming_ref = bf16[8,7,32,128]{3,2,1,0:T(8,128)(2,1)S(1)} all-to-all(bf16[8,7,32,128]{3,2,1,0:T(8,128)(2,1)S(1)} %get-tuple-element.37), channel_id=1, replica_groups=mesh['z_far'=8,'z_near'=2,'x'=4,'core'=2,'tp'=4] {'z_near','x'}, dimensions={0} | all-to-all | bytes 917504 | tf_op jit(solution)/shard_map/cond/branch_0_fun/all_to_all | solution.py:298
  51.2 0.8 %attend.2 = bf16[4,2,128,128]{3,2,1,0:T(8,128)(2,1)S(1)} custom-call(s32[4,8]{1,0:T(4,128)S(4)} %get-tuple-element.32.choice_ref, f32[4]{0:T(128)S(4)} %get-tuple-element.33.slope_ref, s32[8,1,128]{2,1,0:T(1,128)S(4)} %get-tuple-element.34.rank_ref, bf16[128,256]{1,0:T(8,128)(2,1)S(1)} %get-tuple-element.35.queries_ref, ...), custom_call_target="tpu_custom_call" | custom-call | tf_op jit(solution)/shard_map/cond/branch_0_fun/attend/pallas_call | solution.py:299
  52.0 9.9 %all_to_all.20.attended_ref = bf16[4,2,128,128]{3,2,1,0:T(8,128)(2,1)S(1)} all-to-all(bf16[4,2,128,128]{3,2,1,0:T(8,128)(2,1)S(1)} %get-tuple-element.61), channel_id=1, replica_groups=mesh['z_far'=8,'z_near'=2,'x'=4,'core'=2,'tp'=4] {'tp'}, dimensions={0} | all-to-all | bytes 524288 | tf_op jit(solution)/shard_map/all_to_all | solution.py:329
  62.0 0.0 copy-done
  62.0 1.0 %mix.1 = bf16[128,512]{1,0:T(8,128)(2,1)} custom-call(bf16[4,2,128,128]{3,2,1,0:T(8,128)(2,1)S(1)} %all_to_all.20.attended_ref, bf16[1024,512]{1,0:T(8,128)(2,1)S(1)} %copy-done), custom_call_target="tpu_custom_call" | custom-call | tf_op jit(solution)/shard_map/mix/pallas_call | solution.py:331
Async XLA Ops:
  2.0 32.2 %all-to-all-start.2 = ((s32[8,1,128]{2,1,0:T(1,128)}), s32[8,1,128]{2,1,0:T(1,128)S(1)}, u32[]{:S(2)}, u32[]{:S(2)}) async-start(s32[8,1,128]{2,1,0:T(1,128)} %get-tuple-element.53), calls=%async_computation.2 | async-start | bytes 8192 | tf_op jit(solution)/shard_map/all_to_all | solution.py:281
  34.9 27.1 %copy-start = (bf16[1024,512]{1,0:T(8,128)(2,1)S(1)}, bf16[1024,512]{1,0:T(8,128)(2,1)}, u32[]{:S(2)}) copy-start(bf16[1024,512]{1,0:T(8,128)(2,1)} %weight_ref.1) | copy-start | bytes 3145732
